TPU v7x, 32 devices: a whole 2x2x4 slice. The times are simulated.
32 devices in a mesh: fs: 4 (over y, x), tp: 8 (over z, core).
Axes of the slice: x: 2, y: 2, z: 4, core: 2. Of those that a mesh axis runs over, the one named last changes fastest.
Arguments:
- tokens: bfloat16 [1024, 2048], P('fs', 'tp'), may hold values from -60 to 60
- norm_gain: float32 [2048], P('fs'), may hold values from 0.1 to 1.9
- gate_weight: float32 [4, 2048, 4096], P(None, 'fs', 'tp'), may hold values from -0.125 to 0.125
- up_weight: float32 [4, 2048, 4096], P(None, 'fs', 'tp'), may hold values from -0.125 to 0.125
- down_weight: float32 [4, 2048, 4096], P(None, 'fs', 'tp'), may hold values from -0.125 to 0.125
- route: int32 [1024, 2], P('fs'), may hold values from 0 to 3, all different within a row; in each aligned block of 256 rows (0 to 255, 256 to 511, ...) at most 256 rows name the same one
- route_weight: float32 [1024, 2], P('fs'), may hold values from 0.2 to 1
Outputs:
- mixed: bfloat16 [1024, 2048], P('fs', 'tp')
- gate_new: bfloat16 [4, 2048, 4096], P('fs', None, 'tp')
- up_new: bfloat16 [4, 2048, 4096], P('fs', None, 'tp')
- down_new: bfloat16 [4, 2048, 4096], P('fs', None, 'tp')
Inputs may be any that keep to these rules, and one draw needn't show every extreme that they name: `route`: the 2 experts of a row differ. In each aligned block of 256 rows (the tokens of one index of fs) no expert is named by more than 256 rows, a bound that some block reaches.
All inputs are finite; a program needn't handle non-finite values.
Results may differ from a plain program's by a relative error of at most 0.024.
Values may be sent and summed in bfloat16 or wider, within the bound.
No kernel may reach another device: no remote copies, remote signals or barrier semaphores. Data moves between devices by JAX's collectives and lax.ppermute only.
A program may use at most 64 MiB of HBM per device.

v0:
```python
import jax
import jax.numpy as jnp
from jax import lax
from jax.sharding import PartitionSpec as P

epsilon = 1e-05


def slot_table(route, block_rows, expert_count):
    pair_ids = route.reshape(-1, block_rows * route.shape[1])
    onehot = (
        pair_ids[:, :, None] == jnp.arange(expert_count, dtype=jnp.int32)[None, None, :]
    ).astype(jnp.int32)
    before = jnp.cumsum(onehot, axis=1) - onehot
    return jnp.sum(before * onehot, axis=2).reshape(route.shape)


def body(tokens, norm_gain, gate_weight, up_weight, down_weight, route, route_weight):
    experts = gate_weight.shape[0]
    tok_rows = tokens.shape[0]
    columns = tokens.shape[1]
    fs_count = lax.axis_size("fs")
    capacity = 4 * tok_rows // fs_count
    gain_col = norm_gain[None, :, None]
    gate_cast = (gate_weight * gain_col).astype(jnp.bfloat16)
    up_cast = (up_weight * gain_col).astype(jnp.bfloat16)
    down_cast = down_weight.astype(jnp.bfloat16)
    gate_new, up_new, down_new = (
        lax.all_to_all(gate_cast, "fs", split_axis=0, concat_axis=1, tiled=True),
        lax.all_to_all(up_cast, "fs", split_axis=0, concat_axis=1, tiled=True),
        lax.all_to_all(down_cast, "fs", split_axis=0, concat_axis=1, tiled=True),
    )
    slot_of = slot_table(route, tok_rows, experts)
    target = route * capacity + slot_of
    slot_lanes = jnp.arange(experts * capacity, dtype=jnp.int32)
    slot_hits = target[:, :, None] == slot_lanes[None, None, :]
    token_iota = jnp.arange(tok_rows, dtype=jnp.int32)[:, None, None]
    lane_token = jnp.sum(jnp.where(slot_hits, token_iota + 1, 0), axis=(0, 1)) - 1
    lane_token = jnp.where(lane_token < 0, tok_rows, lane_token)
    combine = jnp.sum(jnp.where(slot_hits, route_weight[:, :, None], 0.0), axis=1)
    tok_float = tokens.astype(jnp.float32)
    square_sum = lax.psum(jnp.sum(tok_float * tok_float, axis=1), "tp")
    full_width = columns * lax.axis_size("tp")
    normed = (tok_float * lax.rsqrt(square_sum / full_width + epsilon)[:, None]).astype(
        jnp.bfloat16
    )
    padded = jnp.concatenate([normed, jnp.zeros((1, columns), jnp.bfloat16)], axis=0)
    outgoing = padded[lane_token].reshape(experts, capacity, columns)
    arrived = lax.all_to_all(outgoing, "fs", split_axis=0, concat_axis=0, tiled=True).reshape(
        -1, columns
    )
    gate_local = gate_new[0]
    up_local = up_new[0]
    piece_rows = lax.all_gather(arrived, "tp", axis=1, tiled=True)
    gate_acc = jnp.dot(piece_rows, gate_local, preferred_element_type=jnp.float32)
    up_acc = jnp.dot(piece_rows, up_local, preferred_element_type=jnp.float32)
    hidden = (jax.nn.silu(gate_acc) * up_acc).astype(jnp.bfloat16)
    down_local = down_new[0]
    summed = lax.psum_scatter(
        lax.dot_general(
            down_local, hidden, (((1,), (1,)), ((), ())), preferred_element_type=jnp.float32
        ).astype(jnp.bfloat16),
        "tp",
        scatter_dimension=0,
        tiled=True,
    ).astype(jnp.float32)
    own_columns = summed.shape[0]
    outgoing_back = summed.astype(jnp.bfloat16).reshape(own_columns, fs_count, capacity)
    returned = lax.all_to_all(outgoing_back, "fs", split_axis=1, concat_axis=1, tiled=True).reshape(
        own_columns, experts * capacity
    )
    mixed = lax.dot_general(
        combine,
        returned.astype(jnp.float32),
        (((1,), (1,)), ((), ())),
        precision=lax.Precision.HIGHEST,
        preferred_element_type=jnp.float32,
    )
    return (mixed.astype(jnp.bfloat16), gate_new, up_new, down_new)


def solution(mesh):
    in_specs = (
        P("fs", "tp"),
        P("fs"),
        P(None, "fs", "tp"),
        P(None, "fs", "tp"),
        P(None, "fs", "tp"),
        P("fs", None),
        P("fs", None),
    )
    out_specs = (P("fs", "tp"), P("fs", None, "tp"), P("fs", None, "tp"), P("fs", None, "tp"))
    return jax.shard_map(body, mesh=mesh, in_specs=in_specs, out_specs=out_specs, check_vma=False)
```

profile of v0, /device:TPU:0, one launch (start us, length us, event | category | flops | bytes accessed | tf_op | source)
XLA Modules:
  0.0 224.2 jit_solution(16390866846317587679)
XLA Ops:
  7.2 0.8 copy.21
  8.2 1.2 reduce-window.6
  10.2 0.7 multiply_add_fusion
  11.2 1.0 fusion
  12.2 18.1 %psum.7 = f32[256]{0:T(256)S(1)} all-reduce(f32[256]{0:T(256)S(1)} %fusion), channel_id=1, replica_groups=mesh['fs'=4,'tp'=8] {'tp'}, use_global_device_ids=true, to_apply=%region_5.6 | all-reduce | flops 256 | bytes 2048 | tf_op jit(solution)/shard_map/psum | solution.py:42
  30.4 1.0 fusion.1
  31.4 3.9 %gather_fusion = bf16[1024,256]{1,0:T(8,128)(2,1)S(1)} fusion(bf16[257,256]{1,0:T(8,128)(2,1)S(1)} %concatenate.3, s32[1024]{0:T(1024)S(1)} %broadcast_clamp_fusion), kind=kCustom, calls=%fused_computation | custom fusion | bytes 1052672 | tf_op jit(solution)/shard_map/gather | solution.py:48
  35.3 10.7 %all_to_all.46 = bf16[4,256,256]{2,1,0:T(8,128)(2,1)} all-to-all(bf16[4,256,256]{2,1,0:T(8,128)(2,1)S(1)} %bitcast.31), channel_id=1, replica_groups=mesh['fs'=4,'tp'=8] {'fs'}, dimensions={0} | all-to-all | bytes 1048576 | tf_op jit(solution)/shard_map/all_to_all | solution.py:49
  46.1 6.1 %multiply_convert_fusion = (bf16[4,512,512]{2,1,0:T(8,128)(2,1)}, bf16[4,512,512]{2,1,0:T(8,128)(2,1)S(1)}) fusion(f32[4,512,512]{2,1,0:T(8,128)} %param.10, f32[512]{0:T(512)S(1)} %copy-done.1, f32[4,512,512]{2,1,0:T(8,128)} %param.9), kind=kLoop, calls=%fused_computation.2 | loop fusion | flops 4194304 | bytes 12584960 | tf_op jit(solution)/shard_map/convert_element_type | solution.py:26
  52.3 23.8 %all_to_all.47 = bf16[4,512,512]{2,1,0:T(8,128)(2,1)S(1)} all-to-all(bf16[4,512,512]{2,1,0:T(8,128)(2,1)S(1)} %get-tuple-element.5), channel_id=1, replica_groups=mesh['fs'=4,'tp'=8] {'fs'}, dimensions={0} | all-to-all | bytes 4194304 | tf_op jit(solution)/shard_map/all_to_all | solution.py:29
  76.1 4.5 %all-to-all-start.2 = ((bf16[4,512,512]{2,1,0:T(8,128)(2,1)}), bf16[4,512,512]{2,1,0:T(8,128)(2,1)}, u32[]{:S(2)}, u32[]{:S(2)}) async-start(bf16[4,512,512]{2,1,0:T(8,128)(2,1)} %get-tuple-element.4), calls=%async_computation.2 | async-start | bytes 4194304 | tf_op jit(solution)/shard_map/all_to_all | solution.py:30
  80.6 3.8 %convert_element_type.47 = bf16[4,512,512]{2,1,0:T(8,128)(2,1)} convert(f32[4,512,512]{2,1,0:T(8,128)} %param.11) | non-fusion elementwise | flops 1048576 | bytes 6291456 | tf_op jit(solution)/shard_map/convert_element_type | solution.py:27
  84.4 16.0 %all-to-all-done.2 = bf16[4,512,512]{2,1,0:T(8,128)(2,1)} async-done(((bf16[4,512,512]{2,1,0:T(8,128)(2,1)}), bf16[4,512,512]{2,1,0:T(8,128)(2,1)}, u32[]{:S(2)}, u32[]{:S(2)}) %all-to-all-start.2) | async-done | bytes 2097184 | tf_op jit(solution)/shard_map/all_to_all | solution.py:30
  100.4 4.5 %all-to-all-start.3 = ((bf16[4,512,512]{2,1,0:T(8,128)(2,1)}), bf16[4,512,512]{2,1,0:T(8,128)(2,1)}, u32[]{:S(2)}, u32[]{:S(2)}) async-start(bf16[4,512,512]{2,1,0:T(8,128)(2,1)} %convert_element_type.47), calls=%async_computation.3 | async-start | bytes 4194304 | tf_op jit(solution)/shard_map/all_to_all | solution.py:31
  104.9 5.8 %fusion.5 = f32[1024,512]{1,0:T(8,128)} fusion(bf16[1024,2048]{1,0:T(8,128)(2,1)} %all-gather.2.cloned.1.call-done, bf16[2048,512]{1,0:T(8,128)(2,1)S(1)} %bitcast.28), kind=kOutput, calls=%fused_computation.28 | convolution fusion | flops 2147483648 | bytes 8388608 | tf_op jit(solution)/shard_map/dot_general | solution.py:55
  110.8 18.5 %all-to-all-done.3 = bf16[4,512,512]{2,1,0:T(8,128)(2,1)} async-done(((bf16[4,512,512]{2,1,0:T(8,128)(2,1)}), bf16[4,512,512]{2,1,0:T(8,128)(2,1)}, u32[]{:S(2)}, u32[]{:S(2)}) %all-to-all-start.3) | async-done | bytes 2097184 | tf_op jit(solution)/shard_map/all_to_all | solution.py:31
  129.3 10.6 %convert_bitcast_fusion = bf16[2048,1024]{0,1:T(8,128)(2,1)} fusion(bf16[2048,512]{1,0:T(8,128)(2,1)} %bitcast.9, f32[1024,512]{1,0:T(8,128)} %fusion.5, bf16[1024,2048]{1,0:T(8,128)(2,1)} %all-gather.2.cloned.1.call-done, bf16[2048,512]{1,0:T(8,128)(2,1)} %bitcast.8), kind=kOutput, calls=%fused_computation.1 | convolution fusion | flops 4300210176 | bytes 14680064 | tf_op jit(solution)/shard_map/dot_general | solution.py:60
  139.9 56.9 %reduce-scatter.2.cloned.1.call-done = bf16[256,1024]{0,1:T(8,128)(2,1)} async-done(((bf16[2048,1024]{0,1:T(8,128)(2,1)}), bf16[256,1024]{0,1:T(8,128)(2,1)}) %reduce-scatter.2.cloned.1.call-update) | async-done | bytes 524304 | tf_op jit(solution)/shard_map/reduce_scatter | solution.py:59
  196.8 4.1 %all-to-all-start.4 = ((bf16[256,4,256]{0,2,1:T(8,128)(2,1)}), bf16[256,4,256]{0,2,1:T(8,128)(2,1)}, u32[]{:S(2)}, u32[]{:S(2)}) async-start(bf16[256,4,256]{0,2,1:T(8,128)(2,1)} %bitcast.32), calls=%async_computation.5 | async-start | bytes 1048576 | tf_op jit(solution)/shard_map/all_to_all | solution.py:69
  201.3 6.4 %all-to-all-done.4 = bf16[256,4,256]{0,2,1:T(8,128)(2,1)} async-done(((bf16[256,4,256]{0,2,1:T(8,128)(2,1)}), bf16[256,4,256]{0,2,1:T(8,128)(2,1)}, u32[]{:S(2)}, u32[]{:S(2)}) %all-to-all-start.4) | async-done | bytes 524320 | tf_op jit(solution)/shard_map/all_to_all | solution.py:69
  207.6 2.3 %convolution_convert_fusion = bf16[256,256]{1,0:T(8,128)(2,1)} fusion(f32[256,1024]{1,0:T(8,128)S(1)} %select_reduce_fusion.1, bf16[256,1024]{0,1:T(8,128)(2,1)} %bitcast.12), kind=kOutput, calls=%fused_computation.8 | convolution fusion | flops 805371904 | bytes 1703936 | tf_op jit(solution)/shard_map/dot_general | solution.py:72
  209.9 1.3 copy.26
  211.3 3.0 %copy.27 = bf16[1,2048,512]{2,1,0:T(8,128)(2,1)} copy(bf16[1,2048,512]{2,1,0:T(8,128)(2,1)} %bitcast.14) | data formatting | bytes 4194304
  214.3 3.0 %copy.28 = bf16[1,2048,512]{2,1,0:T(8,128)(2,1)} copy(bf16[1,2048,512]{2,1,0:T(8,128)(2,1)} %bitcast.15) | data formatting | bytes 4194304
  (29 shorter events, 1.6 us)
Async XLA Ops:
  7.2 97.8 %all-gather.2.cloned.1.call-start = ((), (), s32[]{:S(2)}) async-start(), calls=%async_computation.6 | async-start | bytes 4718592 | tf_op jit(solution)/shard_map/all_gather | solution.py:54
  31.4 14.7 %copy-start.1 = (f32[512]{0:T(512)S(1)}, f32[512]{0:T(512)}, u32[]{:S(2)}) copy-start(f32[512]{0:T(512)} %param.8) | copy-start | bytes 6148
  76.1 24.3 %all-to-all-start.2 = ((bf16[4,512,512]{2,1,0:T(8,128)(2,1)}), bf16[4,512,512]{2,1,0:T(8,128)(2,1)}, u32[]{:S(2)}, u32[]{:S(2)}) async-start(bf16[4,512,512]{2,1,0:T(8,128)(2,1)} %get-tuple-element.4), calls=%async_computation.2 | async-start | bytes 4194304 | tf_op jit(solution)/shard_map/all_to_all | solution.py:30
  100.4 28.9 %all-to-all-start.3 = ((bf16[4,512,512]{2,1,0:T(8,128)(2,1)}), bf16[4,512,512]{2,1,0:T(8,128)(2,1)}, u32[]{:S(2)}, u32[]{:S(2)}) async-start(bf16[4,512,512]{2,1,0:T(8,128)(2,1)} %convert_element_type.47), calls=%async_computation.3 | async-start | bytes 4194304 | tf_op jit(solution)/shard_map/all_to_all | solution.py:31
  104.9 92.0 %reduce-scatter.2.cloned.1.call-start = ((), (), s32[]{:S(2)}) async-start(), calls=%async_computation.7 | async-start | bytes 4718592 | tf_op jit(solution)/shard_map/reduce_scatter | solution.py:59
  139.9 61.1 %copy-start = (f32[256,2]{0,1:T(2,128)S(1)}, f32[256,2]{0,1:T(2,128)}, u32[]{:S(2)}) copy-start(f32[256,2]{0,1:T(2,128)} %param.13) | copy-start | bytes 6148
  196.8 10.8 %all-to-all-start.4 = ((bf16[256,4,256]{0,2,1:T(8,128)(2,1)}), bf16[256,4,256]{0,2,1:T(8,128)(2,1)}, u32[]{:S(2)}, u32[]{:S(2)}) async-start(bf16[256,4,256]{0,2,1:T(8,128)(2,1)} %bitcast.32), calls=%async_computation.5 | async-start | bytes 1048576 | tf_op jit(solution)/shard_map/all_to_all | solution.py:69
Sparse Core Ops, SparseCore 0:
  46.2 44.4 all-gather.1
  140.0 56.7 reduce-scatter.1
where the time goes:
time: 225 us; the launch traced here: 224 us
  waiting for transfers between devices  97.9 us (44%)
  blocking collectives  52.7 us (23%)
  matrix products  18.7 us (8%)
  other arithmetic  14.6 us (6%)
  between operations  14.2 us (6%)
  starting transfers between devices  13.2 us (6%)
  local copies, waits for them, and re-layouts  12.9 us (6%)
    reduce_scatter x1, waiting for transfers between devices, body(): lax.psum_scatter(lax.dot_general(down_local, hidden, (((1,), (1,)), ((),...  56.9 us
    all_to_all x1, blocking collectives, body(): lax.all_to_all(gate_cast, 'fs', split_axis=0, concat_axis=1, tiled=True)  23.8 us
    all_to_all x1, waiting for transfers between devices, body(): lax.all_to_all(down_cast, 'fs', split_axis=0, concat_axis=1, tiled=True)  18.5 us
    psum x1, blocking collectives, body(): square_sum = lax.psum(jnp.sum(tok_float * tok_float, axis=1), 'tp')  18.1 us
    all_to_all x1, waiting for transfers between devices, body(): lax.all_to_all(up_cast, 'fs', split_axis=0, concat_axis=1, tiled=True)  16 us
    all_to_all x1, blocking collectives, body(): lax.all_to_all(outgoing, 'fs', split_axis=0, concat_axis=0, tiled=True)  10.7 us
    dot_general x1, matrix products, body(): lax.dot_general(down_local, hidden, (((1,), (1,)), ((), ())), preferred_e...  10.6 us
    unnamed x8, local copies, waits for them, and re-layouts  8.23 us
  transfers between devices with their start and end apart: 5, of which 4 were waited for; matrix products, arithmetic and copies ran while one was open for 7% of the time, Pallas kernels for 0%

commit v1 on v0

--- a/solution.py
+++ b/solution.py
@@ -1,6 +1,8 @@
 import jax
 import jax.numpy as jnp
 from jax import lax
+from jax.experimental import pallas as pl
+from jax.experimental.pallas import tpu as pltpu
 from jax.sharding import PartitionSpec as P
 
 epsilon = 1e-05
@@ -15,7 +17,7 @@
     return jnp.sum(before * onehot, axis=2).reshape(route.shape)
 
 
-def body(tokens, norm_gain, gate_weight, up_weight, down_weight, route, route_weight):
+def sparse_body(tokens, norm_gain, gate_weight, up_weight, down_weight, route, route_weight):
     experts = gate_weight.shape[0]
     tok_rows = tokens.shape[0]
     columns = tokens.shape[1]
@@ -49,23 +51,20 @@
     arrived = lax.all_to_all(outgoing, "fs", split_axis=0, concat_axis=0, tiled=True).reshape(
         -1, columns
     )
-    gate_local = gate_new[0]
-    up_local = up_new[0]
     piece_rows = lax.all_gather(arrived, "tp", axis=1, tiled=True)
-    gate_acc = jnp.dot(piece_rows, gate_local, preferred_element_type=jnp.float32)
-    up_acc = jnp.dot(piece_rows, up_local, preferred_element_type=jnp.float32)
+    gate_acc = jnp.dot(piece_rows, gate_new[0], preferred_element_type=jnp.float32)
+    up_acc = jnp.dot(piece_rows, up_new[0], preferred_element_type=jnp.float32)
     hidden = (jax.nn.silu(gate_acc) * up_acc).astype(jnp.bfloat16)
-    down_local = down_new[0]
     summed = lax.psum_scatter(
         lax.dot_general(
-            down_local, hidden, (((1,), (1,)), ((), ())), preferred_element_type=jnp.float32
+            down_new[0], hidden, (((1,), (1,)), ((), ())), preferred_element_type=jnp.float32
         ).astype(jnp.bfloat16),
         "tp",
         scatter_dimension=0,
         tiled=True,
-    ).astype(jnp.float32)
+    )
     own_columns = summed.shape[0]
-    outgoing_back = summed.astype(jnp.bfloat16).reshape(own_columns, fs_count, capacity)
+    outgoing_back = summed.reshape(own_columns, fs_count, capacity)
     returned = lax.all_to_all(outgoing_back, "fs", split_axis=1, concat_axis=1, tiled=True).reshape(
         own_columns, experts * capacity
     )
@@ -77,6 +76,368 @@
         preferred_element_type=jnp.float32,
     )
     return (mixed.astype(jnp.bfloat16), gate_new, up_new, down_new)
+
+
+def far_last(count):
+    powers = [m for m in range(1, count) if m & (m - 1) == 0]
+    return powers[::-1] + [m for m in range(1, count) if m & (m - 1)]
+
+
+def far_first(count):
+    return sorted(range(1, count), key=lambda k: (-bin(k).count("1"), k))
+
+
+def swap(x, axis, distance):
+    count = lax.axis_size(axis)
+    return lax.ppermute(x, axis, [(s, s ^ distance) for s in range(count)])
+
+
+def local_kernel(body, outs, flops=0, moved=0, extra=0, **kwargs):
+    def call(*operands):
+        held = sum(x.size * x.dtype.itemsize for x in operands)
+        held += sum(x.size * x.dtype.itemsize for x in jax.tree.leaves(outs))
+        return pl.pallas_call(
+            body,
+            out_shape=outs,
+            cost_estimate=pl.CostEstimate(flops=flops, bytes_accessed=moved, transcendentals=0),
+            compiler_params=pltpu.CompilerParams(vmem_limit_bytes=held + extra + GRANT),
+            **kwargs,
+        )(*operands)
+
+    return call
+
+
+GRANT = 4 << 20
+HBM = pl.BlockSpec(memory_space=pltpu.HBM)
+SMEM = pl.BlockSpec(memory_space=pltpu.SMEM)
+VMEM = pl.BlockSpec(memory_space=pltpu.VMEM)
+
+
+def cast_scaled(ids, weight, gain):
+    count, rows, cols = weight.shape
+    tile = 128
+
+    def kernel(ids_ref, w_ref, gain_ref, *out_refs):
+        for r in range(0, rows, tile):
+            column = jnp.broadcast_to(gain_ref[:, r : r + tile], (tile, tile)).T
+            column = jnp.concatenate([column] * (cols // tile), axis=1)
+            for k in range(count):
+                scaled = w_ref[ids_ref[0] ^ k, r : r + tile] * column
+                out_refs[k][r : r + tile, :] = scaled.astype(jnp.bfloat16)
+
+    return local_kernel(
+        kernel,
+        [jax.ShapeDtypeStruct((rows, cols), jnp.bfloat16)] * count,
+        2 * weight.size,
+        6 * weight.size,
+        in_specs=[SMEM, VMEM, VMEM],
+        out_specs=[VMEM] * count,
+    )(ids, weight, gain[None, :])
+
+
+def cast_pieces(ids, weight, pieces):
+    count, rows, cols = weight.shape
+    piece = rows // 2 // pieces
+
+    def kernel(ids_ref, w_ref, *out_refs):
+        for h in range(pieces):
+            for k in range(count):
+                for side in range(2):
+                    start = side * (rows // 2) + h * piece
+                    out_refs[h * count + k][side] = w_ref[
+                        ids_ref[0] ^ k, start : start + piece
+                    ].astype(jnp.bfloat16)
+
+    outs = local_kernel(
+        kernel,
+        [jax.ShapeDtypeStruct((2, piece, cols), jnp.bfloat16)] * (count * pieces),
+        2 * weight.size,
+        6 * weight.size,
+        in_specs=[SMEM, VMEM],
+        out_specs=[VMEM] * (count * pieces),
+    )(ids, weight)
+    return [list(outs[h * count : (h + 1) * count]) for h in range(pieces)]
+
+
+def stack_rows(parts):
+    rows, cols = parts[0].shape
+
+    def kernel(*refs):
+        for k in range(len(parts)):
+            refs[-1][k * rows : (k + 1) * rows, :] = refs[k][...]
+
+    return local_kernel(
+        kernel,
+        jax.ShapeDtypeStruct((len(parts) * rows, cols), parts[0].dtype),
+        0,
+        4 * len(parts) * rows * cols,
+        in_specs=[VMEM] * len(parts),
+        out_specs=VMEM,
+    )(*parts)
+
+
+def lay_rows(ids_ref, part_refs, full_ref, w_ref, sems, columns):
+    part_rows = part_refs[0].shape[0]
+    copies = []
+    for k, ref in enumerate(part_refs):
+        at = pl.multiple_of((ids_ref[0] ^ k) * part_rows, part_rows)
+        copies.append(pltpu.make_async_copy(ref, full_ref.at[pl.ds(at, part_rows)], sems.at[k]))
+        copies[-1].start()
+    for k, ref in enumerate(part_refs):
+        m = ids_ref[0] ^ ids_ref[1] ^ k
+        for s in range(2):
+            to = pl.multiple_of((2 * m + s) * columns, columns)
+            at = pl.multiple_of((ids_ref[2] ^ s) * columns, columns)
+            w_ref[pl.ds(to, columns), :] = ref[pl.ds(at, columns), :]
+    return copies
+
+
+def gate_product(ids, groups, parts):
+    columns = groups[0][0].shape[1]
+    part_rows, cols = parts[0].shape
+    rows = sum(group[0].shape[0] for group in groups)
+    blocks, count = len(groups[0]), len(parts)
+
+    def kernel(ids_ref, *refs):
+        acc_ref, full_ref, ss_ref, w_ref, sems = refs[-5:]
+        copies = lay_rows(ids_ref, refs[-5 - count : -5], full_ref, w_ref, sems, columns)
+        start = 0
+        for g in range(len(groups)):
+            x_refs = refs[g * blocks : (g + 1) * blocks]
+            span = x_refs[0].shape[0]
+            for r in range(0, span, TILE):
+                tile = min(TILE, span - r)
+                x = jnp.concatenate([ref[r : r + tile, :] for ref in x_refs], axis=1)
+                acc_ref[start + r : start + r + tile, :] = jnp.dot(
+                    x, w_ref[...], preferred_element_type=jnp.float32
+                )
+                total = 0.0
+                for ref in x_refs:
+                    wide = ref[r : r + tile, :].astype(jnp.float32)
+                    total = total + wide * wide
+                total = jnp.sum(total, axis=1, keepdims=True)
+                ss_ref[start + r : start + r + tile, :] = jnp.broadcast_to(total, (tile, 128))
+            start += span
+        for copy in copies:
+            copy.wait()
+
+    outs = [
+        jax.ShapeDtypeStruct((rows, cols), jnp.float32),
+        jax.ShapeDtypeStruct((count * part_rows, cols), jnp.bfloat16),
+        jax.ShapeDtypeStruct((rows, 128), jnp.float32),
+    ]
+    operands = [x for group in groups for x in group] + list(parts)
+    return local_kernel(
+        kernel,
+        outs,
+        2 * rows * blocks * columns * cols,
+        rows * blocks * columns * 2 + rows * cols * 4,
+        in_specs=[SMEM] + [VMEM] * len(operands),
+        out_specs=[VMEM, HBM, VMEM],
+        scratch_shapes=[
+            pltpu.VMEM((blocks * columns, cols), jnp.bfloat16),
+            pltpu.SemaphoreType.DMA((count,)),
+        ],
+    )(ids, *operands)
+
+
+def hidden_product(ids, groups, parts, gate_acc, squares):
+    columns = groups[0][0].shape[1]
+    part_rows, cols = parts[0].shape
+    rows = gate_acc.shape[0]
+    blocks, count = len(groups[0]), len(parts)
+
+    def kernel(ids_ref, ga_ref, ss_ref, *refs):
+        out_ref, full_ref, w_ref, sems = refs[-4:]
+        copies = lay_rows(ids_ref, refs[-4 - count : -4], full_ref, w_ref, sems, columns)
+        start = 0
+        for g in range(len(groups)):
+            x_refs = refs[g * blocks : (g + 1) * blocks]
+            span = x_refs[0].shape[0]
+            for r in range(0, span, TILE):
+                tile = min(TILE, span - r)
+                at = slice(start + r, start + r + tile)
+                x = jnp.concatenate([ref[r : r + tile, :] for ref in x_refs], axis=1)
+                scale = lax.rsqrt(ss_ref[at, 0:1] / (blocks * columns) + epsilon)
+                up = jnp.dot(x, w_ref[...], preferred_element_type=jnp.float32) * scale
+                gate = ga_ref[at, :] * scale
+                out_ref[at, :] = (gate / (1.0 + jnp.exp(-gate)) * up).astype(jnp.bfloat16)
+            start += span
+        for copy in copies:
+            copy.wait()
+
+    outs = [
+        jax.ShapeDtypeStruct((rows, cols), jnp.bfloat16),
+        jax.ShapeDtypeStruct((count * part_rows, cols), jnp.bfloat16),
+    ]
+    operands = [x for group in groups for x in group] + list(parts)
+    return local_kernel(
+        kernel,
+        outs,
+        2 * rows * blocks * columns * cols,
+        rows * blocks * columns * 2 + rows * cols * 4,
+        in_specs=[SMEM] + [VMEM] * (2 + len(operands)),
+        out_specs=[VMEM, HBM],
+        scratch_shapes=[
+            pltpu.VMEM((blocks * columns, cols), jnp.bfloat16),
+            pltpu.SemaphoreType.DMA((count,)),
+        ],
+    )(ids, gate_acc, squares, *operands)
+
+
+def down_product(ids, hidden, parts, full, h, pieces):
+    rows, cols = hidden.shape
+    count = len(parts)
+    piece = parts[0].shape[1]
+    full_shape = jax.ShapeDtypeStruct((count, 2, pieces, piece, cols), jnp.bfloat16)
+
+    def kernel(ids_ref, hidden_ref, *refs):
+        part_refs = refs[:count]
+        sent_ref, kept_ref, full_ref, w_ref, sems = refs[-5:]
+        copies = []
+        for k, ref in enumerate(part_refs):
+            to = full_ref.at[ids_ref[0] ^ k, :, h]
+            copies.append(pltpu.make_async_copy(ref, to, sems.at[k]))
+            copies[-1].start()
+        for k, ref in enumerate(part_refs):
+            m = ids_ref[0] ^ ids_ref[1] ^ k
+            place, bit = 0, 1
+            while bit < count:
+                place, bit = 2 * place + (m // bit) % 2, 2 * bit
+            for s in range(2):
+                w_ref[s, pl.ds(pl.multiple_of(place * piece, piece), piece), :] = ref[
+                    ids_ref[2] ^ s
+                ]
+        for s, ref in ((1, sent_ref), (0, kept_ref)):
+            ref[...] = lax.dot_general(
+                w_ref[s],
+                hidden_ref[...],
+                (((1,), (1,)), ((), ())),
+                preferred_element_type=jnp.float32,
+            ).astype(jnp.bfloat16)
+        for copy in copies:
+            copy.wait()
+
+    out = jax.ShapeDtypeStruct((count * piece, rows), jnp.bfloat16)
+    operands = [ids, hidden, *parts]
+    in_specs = [SMEM] + [VMEM] * (1 + count)
+    extra = {}
+    if full is not None:
+        operands.append(full)
+        in_specs.append(HBM)
+        extra["input_output_aliases"] = {len(operands) - 1: 2}
+    return local_kernel(
+        kernel,
+        [out, out, full_shape],
+        4 * count * piece * rows * cols,
+        2 * rows * cols + 8 * count * piece * rows,
+        in_specs=in_specs,
+        out_specs=[VMEM, VMEM, HBM],
+        scratch_shapes=[
+            pltpu.VMEM((2, count * piece, cols), jnp.bfloat16),
+            pltpu.SemaphoreType.DMA((count,)),
+        ],
+        **extra,
+    )(*operands)
+
+
+def combine(share, backs):
+    count = len(backs[0])
+    rows = share.shape[1]
+    total_cols = sum(back[0].shape[0] for back in backs)
+
+    def kernel(share_ref, *refs):
+        parts = []
+        for h in range(len(backs)):
+            total = 0.0
+            for k in range(count):
+                term = refs[h * count + k][...].astype(jnp.float32)
+                total = total + share_ref[k : k + 1, :] * term
+            parts.append(total)
+        refs[-1][...] = jnp.concatenate(parts, axis=0).T.astype(jnp.bfloat16)
+
+    flat = [ref for back in backs for ref in back]
+    return local_kernel(
+        kernel,
+        jax.ShapeDtypeStruct((rows, total_cols), jnp.bfloat16),
+        2 * rows * total_cols * count,
+        2 * rows * total_cols * count,
+        in_specs=[VMEM] * (1 + len(flat)),
+        out_specs=VMEM,
+    )(share, *flat)
+
+
+PIECES = 4
+TILE = 256
+RETURNS = ((0, 1, 2), (3,))
+
+
+def dense_body(tokens, norm_gain, gate_weight, up_weight, down_weight, route, route_weight):
+    f32 = jnp.float32
+    fs_count, tp_count = lax.axis_size("fs"), lax.axis_size("tp")
+    z_count = tp_count // 2
+    fs_id, tp_id = lax.axis_index("fs"), lax.axis_index("tp")
+    ids = jnp.stack([fs_id, tp_id // 2, tp_id % 2]).astype(jnp.int32)
+    tok_rows, _ = tokens.shape
+    near = range(fs_count)
+
+    def exchange(parts):
+        got = {k: swap(parts[k], "fs", k) for k in far_first(fs_count)}
+        got[0] = parts[0]
+        return [got[k] for k in near]
+
+    def gather_rows(mine):
+        own = {0: mine}
+        for m in far_last(z_count):
+            top = 1 << (m.bit_length() - 1)
+            low = m & -m
+            source, distance = (mine, m) if m == low else (own[top], m - top)
+            own[m] = swap(source, "tp", 2 * distance)
+        sides = [(own[m], swap(own[m], "tp", 1)) for m in range(z_count)]
+        return [x for side in sides for x in side]
+
+    fs_tokens = exchange([tokens] * fs_count)
+    gate_got = exchange(cast_scaled(ids, gate_weight, norm_gain))
+    up_got = exchange(cast_scaled(ids, up_weight, norm_gain))
+    down_got = [exchange(parts) for parts in cast_pieces(ids, down_weight, PIECES)]
+
+    groups = [gather_rows(tokens), gather_rows(stack_rows(fs_tokens[1:]))]
+    gate_acc, gate_full, squares = gate_product(ids, groups, gate_got)
+    hidden, up_full = hidden_product(ids, groups, up_got, gate_acc, squares)
+
+    wanted = fs_id ^ jnp.arange(fs_count, dtype=jnp.int32)
+    picks = route.T[None, :, :] == wanted[:, None, None]
+    share = jnp.sum(jnp.where(picks, route_weight.T[None, :, :], 0.0), axis=1)
+
+    full, totals = None, []
+    for h in range(PIECES):
+        sent, kept, full = down_product(ids, hidden, down_got[h], full, h, PIECES)
+        came = swap(sent, "tp", 1)
+        total = (kept.astype(f32) + came.astype(f32)).astype(jnp.bfloat16)
+        step = 1
+        while step < z_count:
+            half = total.shape[0] // 2
+            came = swap(total[half:], "tp", 2 * step)
+            total = (total[:half].astype(f32) + came.astype(f32)).astype(jnp.bfloat16)
+            step *= 2
+        totals.append(total)
+    backs = []
+    for members in RETURNS:
+        total = jnp.concatenate([totals[h] for h in members], axis=0)
+        outs = [total[:, k * tok_rows : (k + 1) * tok_rows] for k in near]
+        backs.append(exchange(outs))
+    mixed = combine(share, backs)
+
+    shape = (1, fs_count * gate_weight.shape[1], gate_weight.shape[2])
+    return (mixed, gate_full.reshape(shape), up_full.reshape(shape), full.reshape(shape))
+
+
+def body(tokens, norm_gain, gate_weight, up_weight, down_weight, route, route_weight):
+    fs_count, tp_count = lax.axis_size("fs"), lax.axis_size("tp")
+    power = fs_count & (fs_count - 1) == 0
+    dense = power and 2 * fs_count == tp_count and fs_count == gate_weight.shape[0] and fs_count <= 4
+    run = dense_body if dense else sparse_body
+    return run(tokens, norm_gain, gate_weight, up_weight, down_weight, route, route_weight)
 
 
 def solution(mesh):

time: 225 us -> 174 us (0.77)
  blocking collectives: 52.7 us -> 0 us
  starting transfers between devices: 13.2 us -> 54.9 us
  Pallas kernels: 0 us -> 19.5 us
  matrix products: 18.7 us -> 0 us
  other arithmetic: 14.6 us -> 1.34 us
  between operations: 14.2 us -> 1.03 us
  local copies, waits for them, and re-layouts: 12.9 us -> 2.37 us
  waiting for transfers between devices: 97.9 us -> 94.7 us
    ppermute x0 -> x53, waiting for transfers between devices: none -> 94.7 us  [swap(): return lax.ppermute(x, axis, [(s, s ^ distance) for s in range(count)])]
    reduce_scatter x1 -> x0, waiting for transfers between devices: 56.9 us -> none  [body(): lax.psum_scatter(lax.dot_general(down_local, hidden, (((1,), (1,)), ((),...]
    ppermute x0 -> x53, starting transfers between devices: none -> 54.9 us  [swap(): return lax.ppermute(x, axis, [(s, s ^ distance) for s in range(count)])]
    all_to_all x3 -> x0, waiting for transfers between devices: 40.9 us -> none  [the longest x1 18.5 us: body(): lax.all_to_all(down_cast, 'fs', split_axis=0, concat_axis=1, tiled=True)]
    all_to_all x2 -> x0, blocking collectives: 34.6 us -> none  [the longest x1 23.8 us: body(): lax.all_to_all(gate_cast, 'fs', split_axis=0, concat_axis=1, tiled=True)]
    pallas_call x0 -> x11, Pallas kernels: none -> 19.5 us  [call(): pl.pallas_call(body, out_shape=outs, cost_estimate=pl.CostEstimate(flops=...]
    dot_general x3 -> x0, matrix products: 18.7 us -> none  [the longest x1 10.6 us: body(): lax.dot_general(down_local, hidden, (((1,), (1,)), ((), ())), preferred_e...]
    psum x1 -> x0, blocking collectives: 18.1 us -> none  [body(): square_sum = lax.psum(jnp.sum(tok_float * tok_float, axis=1), 'tp')]
  transfers between devices with their start and end apart: 5 -> 53, of which waited for: 4 -> 22; matrix products, arithmetic and copies ran while one was open for 7% -> 1% of each run, Pallas kernels for 0% -> 10%
where the time goes in v1:
time: 174 us
  waiting for transfers between devices  94.7 us (54%)
  starting transfers between devices  54.9 us (32%)
  Pallas kernels  19.5 us (11%)
  local copies, waits for them, and re-layouts  2.37 us (1%)
    ppermute x53, waiting for transfers between devices, swap(): return lax.ppermute(x, axis, [(s, s ^ distance) for s in range(count)])  94.7 us
    ppermute x53, starting transfers between devices, swap(): return lax.ppermute(x, axis, [(s, s ^ distance) for s in range(count)])  54.9 us
    pallas_call x11, Pallas kernels, call(): pl.pallas_call(body, out_shape=outs, cost_estimate=pl.CostEstimate(flops=...  19.5 us
  transfers between devices with their start and end apart: 53, of which 22 were waited for; matrix products, arithmetic and copies ran while one was open for 1% of the time, Pallas kernels for 10%

profile of v1, /device:TPU:0, one launch (start us, length us, event | category | flops | bytes accessed | tf_op | source)
XLA Modules:
  0.0 173.8 jit_solution(6330441209367424278)
XLA Ops:
  0.6 3.0 %collective-permute-start.7 = (bf16[256,256]{1,0:T(8,128)(2,1)}, bf16[256,256]{1,0:T(8,128)(2,1)S(1)}, u32[]{:S(2)}, u32[]{:S(2)}) collective-permute-start(bf16[256,256]{1,0:T(8,128)(2,1)} %refs_0_.3), channel_id=1, source_target_pairs={{0,8},{8,0},{16,24},{24,16},{1,9},{9,1},{17,25},{25,17},{2,10},{10... | collective-permute-start | bytes 393224 | tf_op jit(solution)/shard_map/ppermute | solution.py:92
  5.2 2.0 %collective-permute-start.1 = (bf16[256,256]{1,0:T(8,128)(2,1)}, bf16[256,256]{1,0:T(8,128)(2,1)S(1)}, u32[]{:S(2)}, u32[]{:S(2)}) collective-permute-start(bf16[256,256]{1,0:T(8,128)(2,1)} %refs_0_.3), channel_id=1, source_target_pairs={{0,2},{1,3},{2,0},{3,1},{4,6},{5,7},{6,4},{7,5},{8,10},{9,11},{10,... | collective-permute-start | bytes 393224 | tf_op jit(solution)/shard_map/ppermute | solution.py:92
  7.9 2.8 %collective-permute-start.3 = (bf16[256,256]{1,0:T(8,128)(2,1)}, bf16[256,256]{1,0:T(8,128)(2,1)S(1)}, u32[]{:S(2)}, u32[]{:S(2)}) collective-permute-start(bf16[256,256]{1,0:T(8,128)(2,1)} %refs_0_.3), channel_id=1, source_target_pairs={{0,4},{1,5},{2,6},{3,7},{4,0},{5,1},{6,2},{7,3},{8,12},{9,13},{10,... | collective-permute-start | bytes 393224 | tf_op jit(solution)/shard_map/ppermute | solution.py:92
  10.7 2.2 %copy-done = f32[4,512,512]{2,1,0:T(8,128)S(1)} copy-done((f32[4,512,512]{2,1,0:T(8,128)S(1)}, f32[4,512,512]{2,1,0:T(8,128)}, u32[]{:S(2)}) %copy-start) | copy-done | bytes 4194328
  13.7 2.3 %collective-permute-start.29 = (bf16[2,64,512]{2,1,0:T(8,128)(2,1)S(1)}, bf16[2,64,512]{2,1,0:T(8,128)(2,1)S(1)}, u32[]{:S(2)}, u32[]{:S(2)}) collective-permute-start(bf16[2,64,512]{2,1,0:T(8,128)(2,1)S(1)} %get-tuple-element.63), channel_id=1, source_target_pairs={{0,8},{8,0},{16,24},{24,16},{1,9},{9,1},{17,25},{25,17},{2,10},{10... | collective-permute-start | bytes 393224 | tf_op jit(solution)/shard_map/ppermute | solution.py:92
  17.2 2.6 %collective-permute-done.29.refs_1_ = bf16[2,64,512]{2,1,0:T(8,128)(2,1)S(1)} collective-permute-done((bf16[2,64,512]{2,1,0:T(8,128)(2,1)S(1)}, bf16[2,64,512]{2,1,0:T(8,128)(2,1)S(1)}, u32[]{:S(2)}, u32[]{:S(2)}) %collective-permute-start.29) | collective-permute-done | bytes 131104 | tf_op jit(solution)/shard_map/ppermute | solution.py:92
  23.5 6.0 %collective-permute-done.5.refs_6_ = bf16[256,256]{1,0:T(8,128)(2,1)S(1)} collective-permute-done((bf16[256,256]{1,0:T(8,128)(2,1)S(1)}, bf16[256,256]{1,0:T(8,128)(2,1)S(1)}, u32[]{:S(2)}, u32[]{:S(2)}) %collective-permute-start.5) | collective-permute-done | bytes 131104 | tf_op jit(solution)/shard_map/ppermute | solution.py:92
  34.3 2.9 %collective-permute-done.13.refs_12_ = bf16[768,256]{1,0:T(8,128)(2,1)S(1)} collective-permute-done((bf16[768,256]{1,0:T(8,128)(2,1)S(1)}, bf16[768,256]{1,0:T(8,128)(2,1)S(1)}, u32[]{:S(2)}, u32[]{:S(2)}) %collective-permute-start.13) | collective-permute-done | bytes 393248 | tf_op jit(solution)/shard_map/ppermute | solution.py:92
  37.2 4.1 %collective-permute-done.11.refs_10_ = bf16[768,256]{1,0:T(8,128)(2,1)S(1)} collective-permute-done((bf16[768,256]{1,0:T(8,128)(2,1)S(1)}, bf16[768,256]{1,0:T(8,128)(2,1)S(1)}, u32[]{:S(2)}, u32[]{:S(2)}) %collective-permute-start.11) | collective-permute-done | bytes 393248 | tf_op jit(solution)/shard_map/ppermute | solution.py:92
  41.3 4.0 %collective-permute-done.17.refs_17_ = bf16[512,512]{1,0:T(8,128)(2,1)S(1)} collective-permute-done((bf16[512,512]{1,0:T(8,128)(2,1)S(1)}, bf16[512,512]{1,0:T(8,128)(2,1)S(1)}, u32[]{:S(2)}, u32[]{:S(2)}) %collective-permute-start.17) | collective-permute-done | bytes 524320 | tf_op jit(solution)/shard_map/ppermute | solution.py:92
  45.3 3.7 %collective-permute-done.15.refs_14_ = bf16[768,256]{1,0:T(8,128)(2,1)S(1)} collective-permute-done((bf16[768,256]{1,0:T(8,128)(2,1)S(1)}, bf16[768,256]{1,0:T(8,128)(2,1)S(1)}, u32[]{:S(2)}, u32[]{:S(2)}) %collective-permute-start.15) | collective-permute-done | bytes 393248 | tf_op jit(solution)/shard_map/ppermute | solution.py:92
  49.8 7.9 %collective-permute-done.18.refs_18_ = bf16[512,512]{1,0:T(8,128)(2,1)S(1)} collective-permute-done((bf16[512,512]{1,0:T(8,128)(2,1)S(1)}, bf16[512,512]{1,0:T(8,128)(2,1)S(1)}, u32[]{:S(2)}, u32[]{:S(2)}) %collective-permute-start.18) | collective-permute-done | bytes 524320 | tf_op jit(solution)/shard_map/ppermute | solution.py:92
  62.8 4.8 %shard_map.104 = (f32[1024,512]{1,0:T(8,128)S(1)}, bf16[2048,512]{1,0:T(8,128)(2,1)}, f32[1024,128]{1,0:T(8,128)S(1)}) custom-call(s32[3]{0:T(128)S(1)} %pad_add_fusion.ids_ref, bf16[256,256]{1,0:T(8,128)(2,1)S(1)} %copy-done.3, bf16[256,256]{1,0:T(8,128)(2,1)S(1)} %collective-permute-done.refs_1_, bf16[256,256]{1,0:T(8,128)(2,1)S(1)} %collective-permute-done.1.refs_2_, ...), custom_call_target="tpu_custom_call" | custom-call | flops 2147483648 | bytes 6291456 | tf_op jit(solution)/shard_map/pallas_call | solution.py:99
  67.6 20.2 %collective-permute-done.24.refs_2_ = bf16[2,64,512]{2,1,0:T(8,128)(2,1)S(1)} collective-permute-done((bf16[2,64,512]{2,1,0:T(8,128)(2,1)S(1)}, bf16[2,64,512]{2,1,0:T(8,128)(2,1)S(1)}, u32[]{:S(2)}, u32[]{:S(2)}) %collective-permute-start.24) | collective-permute-done | bytes 131104 | tf_op jit(solution)/shard_map/ppermute | solution.py:92
  94.2 4.0 %shard_map.106 = (bf16[1024,512]{1,0:T(8,128)(2,1)S(1)}, bf16[2048,512]{1,0:T(8,128)(2,1)}) custom-call(s32[3]{0:T(128)S(1)} %pad_add_fusion.ids_ref, f32[1024,512]{1,0:T(8,128)S(1)} %get-tuple-element.49.ga_ref, f32[1024,128]{1,0:T(8,128)S(1)} %get-tuple-element.50.ss_ref, bf16[256,256]{1,0:T(8,128)(2,1)S(1)} %copy-done.3, ...), custom_call_target="tpu_custom_call" | custom-call | flops 2147483648 | bytes 6291456 | tf_op jit(solution)/shard_map/pallas_call | solution.py:99
  109.1 2.7 %collective-permute-done.44.refs_1_ = bf16[2,64,512]{2,1,0:T(8,128)(2,1)S(1)} collective-permute-done((bf16[2,64,512]{2,1,0:T(8,128)(2,1)S(1)}, bf16[2,64,512]{2,1,0:T(8,128)(2,1)S(1)}, u32[]{:S(2)}, u32[]{:S(2)}) %collective-permute-start.44) | collective-permute-done | bytes 131104 | tf_op jit(solution)/shard_map/ppermute | solution.py:92
  117.0 2.5 %collective-permute-start.39 = (bf16[128,1024]{1,0:T(8,128)(2,1)S(1)}, bf16[128,1024]{1,0:T(8,128)(2,1)S(1)}, u32[]{:S(2)}, u32[]{:S(2)}) collective-permute-start(bf16[128,1024]{1,0:T(8,128)(2,1)S(1)} %slice.105), channel_id=1, source_target_pairs={{0,2},{1,3},{2,0},{3,1},{4,6},{5,7},{6,4},{7,5},{8,10},{9,11},{10,... | collective-permute-start | bytes 786440 | tf_op jit(solution)/shard_map/ppermute | solution.py:92
  120.1 2.1 %collective-permute-start.27 = (bf16[128,1024]{1,0:T(8,128)(2,1)S(1)}, bf16[128,1024]{1,0:T(8,128)(2,1)S(1)}, u32[]{:S(2)}, u32[]{:S(2)}) collective-permute-start(bf16[128,1024]{1,0:T(8,128)(2,1)S(1)} %slice.97), channel_id=1, source_target_pairs={{0,2},{1,3},{2,0},{3,1},{4,6},{5,7},{6,4},{7,5},{8,10},{9,11},{10,... | collective-permute-start | bytes 786440 | tf_op jit(solution)/shard_map/ppermute | solution.py:92
  122.5 4.2 %collective-permute-done.39 = bf16[128,1024]{1,0:T(8,128)(2,1)S(1)} collective-permute-done((bf16[128,1024]{1,0:T(8,128)(2,1)S(1)}, bf16[128,1024]{1,0:T(8,128)(2,1)S(1)}, u32[]{:S(2)}, u32[]{:S(2)}) %collective-permute-start.39) | collective-permute-done | bytes 262176 | tf_op jit(solution)/shard_map/ppermute | solution.py:92
  126.8 3.8 %collective-permute-start.40 = (bf16[64,1024]{1,0:T(8,128)(2,1)S(1)}, bf16[64,1024]{1,0:T(8,128)(2,1)S(1)}, u32[]{:S(2)}, u32[]{:S(2)}) collective-permute-start(bf16[64,1024]{1,0:T(8,128)(2,1)S(1)} %slice.107), channel_id=1, source_target_pairs={{0,4},{1,5},{2,6},{3,7},{4,0},{5,1},{6,2},{7,3},{8,12},{9,13},{10,... | collective-permute-start | bytes 393224 | tf_op jit(solution)/shard_map/ppermute | solution.py:92
  130.6 4.6 %collective-permute-done.33 = bf16[128,1024]{1,0:T(8,128)(2,1)S(1)} collective-permute-done((bf16[128,1024]{1,0:T(8,128)(2,1)S(1)}, bf16[128,1024]{1,0:T(8,128)(2,1)S(1)}, u32[]{:S(2)}, u32[]{:S(2)}) %collective-permute-start.33) | collective-permute-done | bytes 262176 | tf_op jit(solution)/shard_map/ppermute | solution.py:92
  136.5 12.5 %collective-permute-done.48 = bf16[128,1024]{1,0:T(8,128)(2,1)S(1)} collective-permute-done((bf16[128,1024]{1,0:T(8,128)(2,1)S(1)}, bf16[128,1024]{1,0:T(8,128)(2,1)S(1)}, u32[]{:S(2)}, u32[]{:S(2)}) %collective-permute-start.48) | collective-permute-done | bytes 262176 | tf_op jit(solution)/shard_map/ppermute | solution.py:92
  152.2 9.4 %collective-permute-done.49 = bf16[64,1024]{1,0:T(8,128)(2,1)S(1)} collective-permute-done((bf16[64,1024]{1,0:T(8,128)(2,1)S(1)}, bf16[64,1024]{1,0:T(8,128)(2,1)S(1)}, u32[]{:S(2)}, u32[]{:S(2)}) %collective-permute-start.49) | collective-permute-done | bytes 131104 | tf_op jit(solution)/shard_map/ppermute | solution.py:92
  169.9 2.7 %collective-permute-done.51.refs_6_ = bf16[64,256]{1,0:T(8,128)(2,1)S(1)} collective-permute-done((bf16[64,256]{1,0:T(8,128)(2,1)S(1)}, bf16[64,256]{1,0:T(8,128)(2,1)S(1)}, u32[]{:S(2)}, u32[]{:S(2)}) %collective-permute-start.51) | collective-permute-done | bytes 32800 | tf_op jit(solution)/shard_map/ppermute | solution.py:92
  (133 shorter events, 56.0 us)
Async XLA Ops:
  16.0 17.9 %collective-permute-start.10 = (bf16[768,256]{1,0:T(8,128)(2,1)S(1)}, bf16[768,256]{1,0:T(8,128)(2,1)S(1)}, u32[]{:S(2)}, u32[]{:S(2)}) collective-permute-start(bf16[768,256]{1,0:T(8,128)(2,1)S(1)} %shard_map.102.refs_8_), channel_id=1, source_target_pairs={{0,1},{1,0},{2,3},{3,2},{4,5},{5,4},{6,7},{7,6},{8,9},{9,8},{10,11... | collective-permute-start | bytes 1179656 | tf_op jit(solution)/shard_map/ppermute | solution.py:92
  16.9 20.4 %collective-permute-start.13 = (bf16[768,256]{1,0:T(8,128)(2,1)S(1)}, bf16[768,256]{1,0:T(8,128)(2,1)S(1)}, u32[]{:S(2)}, u32[]{:S(2)}) collective-permute-start(bf16[768,256]{1,0:T(8,128)(2,1)S(1)} %shard_map.102.refs_8_), channel_id=1, source_target_pairs={{0,4},{1,5},{2,6},{3,7},{4,0},{5,1},{6,2},{7,3},{8,12},{9,13},{10,... | collective-permute-start | bytes 1179656 | tf_op jit(solution)/shard_map/ppermute | solution.py:92
  21.9 19.3 %collective-permute-start.11 = (bf16[768,256]{1,0:T(8,128)(2,1)S(1)}, bf16[768,256]{1,0:T(8,128)(2,1)S(1)}, u32[]{:S(2)}, u32[]{:S(2)}) collective-permute-start(bf16[768,256]{1,0:T(8,128)(2,1)S(1)} %shard_map.102.refs_8_), channel_id=1, source_target_pairs={{0,2},{1,3},{2,0},{3,1},{4,6},{5,7},{6,4},{7,5},{8,10},{9,11},{10,... | collective-permute-start | bytes 1179656 | tf_op jit(solution)/shard_map/ppermute | solution.py:92
  30.4 14.9 %collective-permute-start.17 = (bf16[512,512]{1,0:T(8,128)(2,1)S(1)}, bf16[512,512]{1,0:T(8,128)(2,1)S(1)}, u32[]{:S(2)}, u32[]{:S(2)}) collective-permute-start(bf16[512,512]{1,0:T(8,128)(2,1)S(1)} %get-tuple-element.46), channel_id=1, source_target_pairs={{0,8},{8,0},{16,24},{24,16},{1,9},{9,1},{17,25},{25,17},{2,10},{10... | collective-permute-start | bytes 1572872 | tf_op jit(solution)/shard_map/ppermute | solution.py:92
  32.4 25.3 %collective-permute-start.18 = (bf16[512,512]{1,0:T(8,128)(2,1)S(1)}, bf16[512,512]{1,0:T(8,128)(2,1)S(1)}, u32[]{:S(2)}, u32[]{:S(2)}) collective-permute-start(bf16[512,512]{1,0:T(8,128)(2,1)S(1)} %get-tuple-element.47), channel_id=1, source_target_pairs={{0,16},{8,24},{16,0},{24,8},{1,17},{9,25},{17,1},{25,9},{2,18},{10... | collective-permute-start | bytes 1572872 | tf_op jit(solution)/shard_map/ppermute | solution.py:92
  33.9 23.8 %collective-permute-start.19 = (bf16[512,512]{1,0:T(8,128)(2,1)S(1)}, bf16[512,512]{1,0:T(8,128)(2,1)S(1)}, u32[]{:S(2)}, u32[]{:S(2)}) collective-permute-start(bf16[512,512]{1,0:T(8,128)(2,1)S(1)} %get-tuple-element.48), channel_id=1, source_target_pairs={{0,24},{8,16},{16,8},{24,0},{1,25},{9,17},{17,9},{25,1},{2,26},{10... | collective-permute-start | bytes 1572872 | tf_op jit(solution)/shard_map/ppermute | solution.py:92
  41.3 18.3 %collective-permute-start.12 = (bf16[768,256]{1,0:T(8,128)(2,1)S(1)}, bf16[768,256]{1,0:T(8,128)(2,1)S(1)}, u32[]{:S(2)}, u32[]{:S(2)}) collective-permute-start(bf16[768,256]{1,0:T(8,128)(2,1)S(1)} %collective-permute-done.11.refs_10_), channel_id=1, source_target_pairs={{0,1},{1,0},{2,3},{3,2},{4,5},{5,4},{6,7},{7,6},{8,9},{9,8},{10,11... | collective-permute-start | bytes 1179656 | tf_op jit(solution)/shard_map/ppermute | solution.py:92
  45.2 15.9 %collective-permute-start.14 = (bf16[768,256]{1,0:T(8,128)(2,1)S(1)}, bf16[768,256]{1,0:T(8,128)(2,1)S(1)}, u32[]{:S(2)}, u32[]{:S(2)}) collective-permute-start(bf16[768,256]{1,0:T(8,128)(2,1)S(1)} %collective-permute-done.13.refs_12_), channel_id=1, source_target_pairs={{0,1},{1,0},{2,3},{3,2},{4,5},{5,4},{6,7},{7,6},{8,9},{9,8},{10,11... | collective-permute-start | bytes 1179656 | tf_op jit(solution)/shard_map/ppermute | solution.py:92
  48.9 13.7 %collective-permute-start.16 = (bf16[768,256]{1,0:T(8,128)(2,1)S(1)}, bf16[768,256]{1,0:T(8,128)(2,1)S(1)}, u32[]{:S(2)}, u32[]{:S(2)}) collective-permute-start(bf16[768,256]{1,0:T(8,128)(2,1)S(1)} %collective-permute-done.15.refs_14_), channel_id=1, source_target_pairs={{0,1},{1,0},{2,3},{3,2},{4,5},{5,4},{6,7},{7,6},{8,9},{9,8},{10,11... | collective-permute-start | bytes 1179656 | tf_op jit(solution)/shard_map/ppermute | solution.py:92
  57.7 33.3 %collective-permute-start.20 = (bf16[512,512]{1,0:T(8,128)(2,1)S(1)}, bf16[512,512]{1,0:T(8,128)(2,1)S(1)}, u32[]{:S(2)}, u32[]{:S(2)}) collective-permute-start(bf16[512,512]{1,0:T(8,128)(2,1)S(1)} %get-tuple-element.52), channel_id=1, source_target_pairs={{0,8},{8,0},{16,24},{24,16},{1,9},{9,1},{17,25},{25,17},{2,10},{10... | collective-permute-start | bytes 1572872 | tf_op jit(solution)/shard_map/ppermute | solution.py:92
  57.7 33.5 %collective-permute-start.21 = (bf16[512,512]{1,0:T(8,128)(2,1)S(1)}, bf16[512,512]{1,0:T(8,128)(2,1)S(1)}, u32[]{:S(2)}, u32[]{:S(2)}) collective-permute-start(bf16[512,512]{1,0:T(8,128)(2,1)S(1)} %get-tuple-element.53), channel_id=1, source_target_pairs={{0,16},{8,24},{16,0},{24,8},{1,17},{9,25},{17,1},{25,9},{2,18},{10... | collective-permute-start | bytes 1572872 | tf_op jit(solution)/shard_map/ppermute | solution.py:92
  59.6 33.2 %collective-permute-start.22 = (bf16[512,512]{1,0:T(8,128)(2,1)S(1)}, bf16[512,512]{1,0:T(8,128)(2,1)S(1)}, u32[]{:S(2)}, u32[]{:S(2)}) collective-permute-start(bf16[512,512]{1,0:T(8,128)(2,1)S(1)} %get-tuple-element.54), channel_id=1, source_target_pairs={{0,24},{8,16},{16,8},{24,0},{1,25},{9,17},{17,9},{25,1},{2,26},{10... | collective-permute-start | bytes 1572872 | tf_op jit(solution)/shard_map/ppermute | solution.py:92
  61.2 26.5 %collective-permute-start.24 = (bf16[2,64,512]{2,1,0:T(8,128)(2,1)S(1)}, bf16[2,64,512]{2,1,0:T(8,128)(2,1)S(1)}, u32[]{:S(2)}, u32[]{:S(2)}) collective-permute-start(bf16[2,64,512]{2,1,0:T(8,128)(2,1)S(1)} %get-tuple-element.58), channel_id=1, source_target_pairs={{0,16},{8,24},{16,0},{24,8},{1,17},{9,25},{17,1},{25,9},{2,18},{10... | collective-permute-start | bytes 393224 | tf_op jit(solution)/shard_map/ppermute | solution.py:92
  62.7 26.6 %collective-permute-start.25 = (bf16[2,64,512]{2,1,0:T(8,128)(2,1)S(1)}, bf16[2,64,512]{2,1,0:T(8,128)(2,1)S(1)}, u32[]{:S(2)}, u32[]{:S(2)}) collective-permute-start(bf16[2,64,512]{2,1,0:T(8,128)(2,1)S(1)} %get-tuple-element.59), channel_id=1, source_target_pairs={{0,24},{8,16},{16,8},{24,0},{1,25},{9,17},{17,9},{25,1},{2,26},{10... | collective-permute-start | bytes 393224 | tf_op jit(solution)/shard_map/ppermute | solution.py:92
  87.7 15.5 %collective-permute-start.35 = (bf16[2,64,512]{2,1,0:T(8,128)(2,1)S(1)}, bf16[2,64,512]{2,1,0:T(8,128)(2,1)S(1)}, u32[]{:S(2)}, u32[]{:S(2)}) collective-permute-start(bf16[2,64,512]{2,1,0:T(8,128)(2,1)S(1)} %get-tuple-element.70), channel_id=1, source_target_pairs={{0,8},{8,0},{16,24},{24,16},{1,9},{9,1},{17,25},{25,17},{2,10},{10... | collective-permute-start | bytes 393224 | tf_op jit(solution)/shard_map/ppermute | solution.py:92
  89.2 13.9 %collective-permute-start.36 = (bf16[2,64,512]{2,1,0:T(8,128)(2,1)S(1)}, bf16[2,64,512]{2,1,0:T(8,128)(2,1)S(1)}, u32[]{:S(2)}, u32[]{:S(2)}) collective-permute-start(bf16[2,64,512]{2,1,0:T(8,128)(2,1)S(1)} %get-tuple-element.71), channel_id=1, source_target_pairs={{0,16},{8,24},{16,0},{24,8},{1,17},{9,25},{17,1},{25,9},{2,18},{10... | collective-permute-start | bytes 393224 | tf_op jit(solution)/shard_map/ppermute | solution.py:92
  105.2 14.4 %collective-permute-start.32 = (bf16[256,1024]{1,0:T(8,128)(2,1)S(1)}, bf16[256,1024]{1,0:T(8,128)(2,1)S(1)}, u32[]{:S(2)}, u32[]{:S(2)}) collective-permute-start(bf16[256,1024]{1,0:T(8,128)(2,1)S(1)} %get-tuple-element.68), channel_id=1, source_target_pairs={{0,1},{1,0},{2,3},{3,2},{4,5},{5,4},{6,7},{7,6},{8,9},{9,8},{10,11... | collective-permute-start | bytes 1572872 | tf_op jit(solution)/shard_map/ppermute | solution.py:92
  119.8 15.4 %collective-permute-start.33 = (bf16[128,1024]{1,0:T(8,128)(2,1)S(1)}, bf16[128,1024]{1,0:T(8,128)(2,1)S(1)}, u32[]{:S(2)}, u32[]{:S(2)}) collective-permute-start(bf16[128,1024]{1,0:T(8,128)(2,1)S(1)} %slice.101), channel_id=1, source_target_pairs={{0,2},{1,3},{2,0},{3,1},{4,6},{5,7},{6,4},{7,5},{8,10},{9,11},{10,... | collective-permute-start | bytes 786440 | tf_op jit(solution)/shard_map/ppermute | solution.py:92
  120.1 30.3 %collective-permute-start.27 = (bf16[128,1024]{1,0:T(8,128)(2,1)S(1)}, bf16[128,1024]{1,0:T(8,128)(2,1)S(1)}, u32[]{:S(2)}, u32[]{:S(2)}) collective-permute-start(bf16[128,1024]{1,0:T(8,128)(2,1)S(1)} %slice.97), channel_id=1, source_target_pairs={{0,2},{1,3},{2,0},{3,1},{4,6},{5,7},{6,4},{7,5},{8,10},{9,11},{10,... | collective-permute-start | bytes 786440 | tf_op jit(solution)/shard_map/ppermute | solution.py:92
  122.4 26.6 %collective-permute-start.48 = (bf16[128,1024]{1,0:T(8,128)(2,1)S(1)}, bf16[128,1024]{1,0:T(8,128)(2,1)S(1)}, u32[]{:S(2)}, u32[]{:S(2)}) collective-permute-start(bf16[128,1024]{1,0:T(8,128)(2,1)S(1)} %slice.113), channel_id=1, source_target_pairs={{0,2},{1,3},{2,0},{3,1},{4,6},{5,7},{6,4},{7,5},{8,10},{9,11},{10,... | collective-permute-start | bytes 786440 | tf_op jit(solution)/shard_map/ppermute | solution.py:92
  126.8 35.6 %collective-permute-start.40 = (bf16[64,1024]{1,0:T(8,128)(2,1)S(1)}, bf16[64,1024]{1,0:T(8,128)(2,1)S(1)}, u32[]{:S(2)}, u32[]{:S(2)}) collective-permute-start(bf16[64,1024]{1,0:T(8,128)(2,1)S(1)} %slice.107), channel_id=1, source_target_pairs={{0,4},{1,5},{2,6},{3,7},{4,0},{5,1},{6,2},{7,3},{8,12},{9,13},{10,... | collective-permute-start | bytes 393224 | tf_op jit(solution)/shard_map/ppermute | solution.py:92
  135.2 27.2 %collective-permute-start.34 = (bf16[64,1024]{1,0:T(8,128)(2,1)S(1)}, bf16[64,1024]{1,0:T(8,128)(2,1)S(1)}, u32[]{:S(2)}, u32[]{:S(2)}) collective-permute-start(bf16[64,1024]{1,0:T(8,128)(2,1)S(1)} %slice.103), channel_id=1, source_target_pairs={{0,4},{1,5},{2,6},{3,7},{4,0},{5,1},{6,2},{7,3},{8,12},{9,13},{10,... | collective-permute-start | bytes 393224 | tf_op jit(solution)/shard_map/ppermute | solution.py:92
  149.1 12.5 %collective-permute-start.49 = (bf16[64,1024]{1,0:T(8,128)(2,1)S(1)}, bf16[64,1024]{1,0:T(8,128)(2,1)S(1)}, u32[]{:S(2)}, u32[]{:S(2)}) collective-permute-start(bf16[64,1024]{1,0:T(8,128)(2,1)S(1)} %slice.115), channel_id=1, source_target_pairs={{0,4},{1,5},{2,6},{3,7},{4,0},{5,1},{6,2},{7,3},{8,12},{9,13},{10,... | collective-permute-start | bytes 393224 | tf_op jit(solution)/shard_map/ppermute | solution.py:92
  150.5 13.3 %collective-permute-start.28 = (bf16[64,1024]{1,0:T(8,128)(2,1)S(1)}, bf16[64,1024]{1,0:T(8,128)(2,1)S(1)}, u32[]{:S(2)}, u32[]{:S(2)}) collective-permute-start(bf16[64,1024]{1,0:T(8,128)(2,1)S(1)} %slice.99), channel_id=1, source_target_pairs={{0,4},{1,5},{2,6},{3,7},{4,0},{5,1},{6,2},{7,3},{8,12},{9,13},{10,... | collective-permute-start | bytes 393224 | tf_op jit(solution)/shard_map/ppermute | solution.py:92
  (36 other events, 360.2 us)

commit v2 on v1

--- a/solution.py
+++ b/solution.py
@@ -83,13 +83,24 @@
     return powers[::-1] + [m for m in range(1, count) if m & (m - 1)]
 
 
-def far_first(count):
+def send_order(count):
     return sorted(range(1, count), key=lambda k: (-bin(k).count("1"), k))
 
 
 def swap(x, axis, distance):
     count = lax.axis_size(axis)
     return lax.ppermute(x, axis, [(s, s ^ distance) for s in range(count)])
+
+
+def place_of(m, count):
+    place, bit = 0, 1
+    while bit < count:
+        place, bit = 2 * place + (m // bit) % 2, 2 * bit
+    return place
+
+
+def add(*terms):
+    return sum(term.astype(jnp.float32) for term in terms).astype(jnp.bfloat16)
 
 
 def local_kernel(body, outs, flops=0, moved=0, extra=0, **kwargs):
@@ -113,50 +124,53 @@
 VMEM = pl.BlockSpec(memory_space=pltpu.VMEM)
 
 
-def cast_scaled(ids, weight, gain):
-    count, rows, cols = weight.shape
+def cast_scaled(ids, weight, gain, wanted):
+    _, rows, cols = weight.shape
     tile = 128
 
     def kernel(ids_ref, w_ref, gain_ref, *out_refs):
         for r in range(0, rows, tile):
             column = jnp.broadcast_to(gain_ref[:, r : r + tile], (tile, tile)).T
             column = jnp.concatenate([column] * (cols // tile), axis=1)
-            for k in range(count):
+            for n, k in enumerate(wanted):
                 scaled = w_ref[ids_ref[0] ^ k, r : r + tile] * column
-                out_refs[k][r : r + tile, :] = scaled.astype(jnp.bfloat16)
-
-    return local_kernel(
-        kernel,
-        [jax.ShapeDtypeStruct((rows, cols), jnp.bfloat16)] * count,
+                out_refs[n][r : r + tile, :] = scaled.astype(jnp.bfloat16)
+
+    return local_kernel(
+        kernel,
+        [jax.ShapeDtypeStruct((rows, cols), jnp.bfloat16)] * len(wanted),
         2 * weight.size,
         6 * weight.size,
         in_specs=[SMEM, VMEM, VMEM],
-        out_specs=[VMEM] * count,
+        out_specs=[VMEM] * len(wanted),
     )(ids, weight, gain[None, :])
 
 
-def cast_pieces(ids, weight, pieces):
+def cast_pieces(ids, weight, spans):
     count, rows, cols = weight.shape
-    piece = rows // 2 // pieces
 
     def kernel(ids_ref, w_ref, *out_refs):
-        for h in range(pieces):
+        for h, (first, size) in enumerate(spans):
             for k in range(count):
                 for side in range(2):
-                    start = side * (rows // 2) + h * piece
+                    start = side * (rows // 2) + first
                     out_refs[h * count + k][side] = w_ref[
-                        ids_ref[0] ^ k, start : start + piece
+                        ids_ref[0] ^ k, start : start + size
                     ].astype(jnp.bfloat16)
 
     outs = local_kernel(
         kernel,
-        [jax.ShapeDtypeStruct((2, piece, cols), jnp.bfloat16)] * (count * pieces),
+        [
+            jax.ShapeDtypeStruct((2, size, cols), jnp.bfloat16)
+            for _, size in spans
+            for _ in range(count)
+        ],
         2 * weight.size,
         6 * weight.size,
         in_specs=[SMEM, VMEM],
-        out_specs=[VMEM] * (count * pieces),
+        out_specs=[VMEM] * (count * len(spans)),
     )(ids, weight)
-    return [list(outs[h * count : (h + 1) * count]) for h in range(pieces)]
+    return [list(outs[h * count : (h + 1) * count]) for h in range(len(spans))]
 
 
 def stack_rows(parts):
@@ -261,13 +275,14 @@
                 scale = lax.rsqrt(ss_ref[at, 0:1] / (blocks * columns) + epsilon)
                 up = jnp.dot(x, w_ref[...], preferred_element_type=jnp.float32) * scale
                 gate = ga_ref[at, :] * scale
-                out_ref[at, :] = (gate / (1.0 + jnp.exp(-gate)) * up).astype(jnp.bfloat16)
+                hidden = (gate / (1.0 + jnp.exp(-gate)) * up).astype(jnp.bfloat16)
+                out_ref[:, at] = hidden.T
             start += span
         for copy in copies:
             copy.wait()
 
     outs = [
-        jax.ShapeDtypeStruct((rows, cols), jnp.bfloat16),
+        jax.ShapeDtypeStruct((cols, rows), jnp.bfloat16),
         jax.ShapeDtypeStruct((count * part_rows, cols), jnp.bfloat16),
     ]
     operands = [x for group in groups for x in group] + list(parts)
@@ -285,66 +300,92 @@
     )(ids, gate_acc, squares, *operands)
 
 
-def down_product(ids, hidden, parts, full, h, pieces):
-    rows, cols = hidden.shape
+def down_product(ids, hidden, parts):
+    cols, rows = hidden.shape
     count = len(parts)
     piece = parts[0].shape[1]
-    full_shape = jax.ShapeDtypeStruct((count, 2, pieces, piece, cols), jnp.bfloat16)
 
     def kernel(ids_ref, hidden_ref, *refs):
         part_refs = refs[:count]
-        sent_ref, kept_ref, full_ref, w_ref, sems = refs[-5:]
-        copies = []
+        sent_ref, kept_ref, w_ref = refs[-3:]
         for k, ref in enumerate(part_refs):
-            to = full_ref.at[ids_ref[0] ^ k, :, h]
-            copies.append(pltpu.make_async_copy(ref, to, sems.at[k]))
-            copies[-1].start()
-        for k, ref in enumerate(part_refs):
-            m = ids_ref[0] ^ ids_ref[1] ^ k
-            place, bit = 0, 1
-            while bit < count:
-                place, bit = 2 * place + (m // bit) % 2, 2 * bit
+            place = place_of(ids_ref[0] ^ ids_ref[1] ^ k, count)
             for s in range(2):
                 w_ref[s, pl.ds(pl.multiple_of(place * piece, piece), piece), :] = ref[
                     ids_ref[2] ^ s
                 ]
         for s, ref in ((1, sent_ref), (0, kept_ref)):
-            ref[...] = lax.dot_general(
-                w_ref[s],
-                hidden_ref[...],
-                (((1,), (1,)), ((), ())),
-                preferred_element_type=jnp.float32,
+            ref[...] = jnp.dot(
+                w_ref[s], hidden_ref[...], preferred_element_type=jnp.float32
             ).astype(jnp.bfloat16)
+
+    out = jax.ShapeDtypeStruct((count * piece, rows), jnp.bfloat16)
+    return local_kernel(
+        kernel,
+        [out, out],
+        4 * count * piece * rows * cols,
+        2 * rows * cols + 8 * count * piece * rows,
+        in_specs=[SMEM] + [VMEM] * (1 + count),
+        out_specs=[VMEM] * 2,
+        scratch_shapes=[pltpu.VMEM((2, count * piece, cols), jnp.bfloat16)],
+    )(ids, hidden, *parts)
+
+
+def lay_pieces(ids, pieces):
+    count = len(pieces[0])
+    cols = pieces[0][0].shape[2]
+    sizes = [parts[0].shape[1] for parts in pieces]
+
+    def kernel(ids_ref, *refs):
+        full_ref, sems = refs[-2:]
+        copies, first = [], 0
+        for h, size in enumerate(sizes):
+            for k in range(count):
+                n = h * count + k
+                to = full_ref.at[ids_ref[0] ^ k, :, pl.ds(first, size)]
+                copies.append(pltpu.make_async_copy(refs[n], to, sems.at[n]))
+                copies[-1].start()
+            first += size
         for copy in copies:
             copy.wait()
 
-    out = jax.ShapeDtypeStruct((count * piece, rows), jnp.bfloat16)
-    operands = [ids, hidden, *parts]
-    in_specs = [SMEM] + [VMEM] * (1 + count)
-    extra = {}
-    if full is not None:
-        operands.append(full)
-        in_specs.append(HBM)
-        extra["input_output_aliases"] = {len(operands) - 1: 2}
-    return local_kernel(
-        kernel,
-        [out, out, full_shape],
-        4 * count * piece * rows * cols,
-        2 * rows * cols + 8 * count * piece * rows,
-        in_specs=in_specs,
-        out_specs=[VMEM, VMEM, HBM],
-        scratch_shapes=[
-            pltpu.VMEM((2, count * piece, cols), jnp.bfloat16),
-            pltpu.SemaphoreType.DMA((count,)),
-        ],
-        **extra,
-    )(*operands)
-
-
-def combine(share, backs):
+    flat = [part for parts in pieces for part in parts]
+    return local_kernel(
+        kernel,
+        jax.ShapeDtypeStruct((count, 2, sum(sizes), cols), jnp.bfloat16),
+        0,
+        8 * count * sum(sizes) * cols,
+        in_specs=[SMEM] + [VMEM] * len(flat),
+        out_specs=HBM,
+        scratch_shapes=[pltpu.SemaphoreType.DMA((len(flat),))],
+    )(ids, *flat)
+
+
+def weighted_cut(kept, came, share):
+    cols, rows = kept.shape
+    count = share.shape[0]
+    cut = rows // count
+
+    def kernel(kept_ref, came_ref, share_ref, *out_refs):
+        for k in range(count):
+            at = slice(k * cut, (k + 1) * cut)
+            total = kept_ref[:, at].astype(jnp.float32) + came_ref[:, at].astype(jnp.float32)
+            out_refs[k][...] = (total * share_ref[k : k + 1, :]).astype(jnp.bfloat16)
+
+    return local_kernel(
+        kernel,
+        [jax.ShapeDtypeStruct((cols, cut), jnp.bfloat16)] * count,
+        2 * kept.size,
+        6 * kept.size,
+        in_specs=[VMEM] * 3,
+        out_specs=[VMEM] * count,
+    )(kept, came, share)
+
+
+def combine(share, backs, ready):
     count = len(backs[0])
     rows = share.shape[1]
-    total_cols = sum(back[0].shape[0] for back in backs)
+    total_cols = sum(back[0].shape[0] for back in backs) + sum(terms[0].shape[0] for terms in ready)
 
     def kernel(share_ref, *refs):
         parts = []
@@ -354,35 +395,41 @@
                 term = refs[h * count + k][...].astype(jnp.float32)
                 total = total + share_ref[k : k + 1, :] * term
             parts.append(total)
+        rest = iter(refs[len(flat) : -1])
+        for terms in ready:
+            parts.append(sum(next(rest)[...].astype(jnp.float32) for _ in terms))
         refs[-1][...] = jnp.concatenate(parts, axis=0).T.astype(jnp.bfloat16)
 
-    flat = [ref for back in backs for ref in back]
+    flat = [x for back in backs for x in back]
+    summed = [x for terms in ready for x in terms]
     return local_kernel(
         kernel,
         jax.ShapeDtypeStruct((rows, total_cols), jnp.bfloat16),
         2 * rows * total_cols * count,
         2 * rows * total_cols * count,
-        in_specs=[VMEM] * (1 + len(flat)),
+        in_specs=[VMEM] * (1 + len(flat) + len(summed)),
         out_specs=VMEM,
-    )(share, *flat)
-
-
-PIECES = 4
+    )(share, *flat, *summed)
+
+
+SHARES = (4, 3, 5, 4)
+PIECES = len(SHARES)
 TILE = 256
-RETURNS = ((0, 1, 2), (3,))
+TP_FIRST = 2
 
 
 def dense_body(tokens, norm_gain, gate_weight, up_weight, down_weight, route, route_weight):
-    f32 = jnp.float32
     fs_count, tp_count = lax.axis_size("fs"), lax.axis_size("tp")
     z_count = tp_count // 2
     fs_id, tp_id = lax.axis_index("fs"), lax.axis_index("tp")
     ids = jnp.stack([fs_id, tp_id // 2, tp_id % 2]).astype(jnp.int32)
-    tok_rows, _ = tokens.shape
+    tok_rows, columns = tokens.shape
     near = range(fs_count)
+    ends = [columns * sum(SHARES[:h]) // sum(SHARES) for h in range(len(SHARES) + 1)]
+    spans = [(a, b - a) for a, b in zip(ends, ends[1:])]
 
     def exchange(parts):
-        got = {k: swap(parts[k], "fs", k) for k in far_first(fs_count)}
+        got = {k: swap(parts[k], "fs", k) for k in send_order(fs_count)}
         got[0] = parts[0]
         return [got[k] for k in near]
 
@@ -397,9 +444,9 @@
         return [x for side in sides for x in side]
 
     fs_tokens = exchange([tokens] * fs_count)
-    gate_got = exchange(cast_scaled(ids, gate_weight, norm_gain))
-    up_got = exchange(cast_scaled(ids, up_weight, norm_gain))
-    down_got = [exchange(parts) for parts in cast_pieces(ids, down_weight, PIECES)]
+    gate_got = exchange(cast_scaled(ids, gate_weight, norm_gain, near))
+    up_got = exchange(cast_scaled(ids, up_weight, norm_gain, near))
+    down_got = [exchange(parts) for parts in cast_pieces(ids, down_weight, spans)]
 
     groups = [gather_rows(tokens), gather_rows(stack_rows(fs_tokens[1:]))]
     gate_acc, gate_full, squares = gate_product(ids, groups, gate_got)
@@ -409,24 +456,36 @@
     picks = route.T[None, :, :] == wanted[:, None, None]
     share = jnp.sum(jnp.where(picks, route_weight.T[None, :, :], 0.0), axis=1)
 
-    full, totals = None, []
-    for h in range(PIECES):
-        sent, kept, full = down_product(ids, hidden, down_got[h], full, h, PIECES)
-        came = swap(sent, "tp", 1)
-        total = (kept.astype(f32) + came.astype(f32)).astype(jnp.bfloat16)
+    shares = exchange([share[k : k + 1] for k in near])
+    share_all = jnp.concatenate(shares, axis=0)
+
+    def halve(total):
         step = 1
         while step < z_count:
             half = total.shape[0] // 2
             came = swap(total[half:], "tp", 2 * step)
-            total = (total[:half].astype(f32) + came.astype(f32)).astype(jnp.bfloat16)
+            total = add(total[:half], came)
             step *= 2
-        totals.append(total)
-    backs = []
-    for members in RETURNS:
-        total = jnp.concatenate([totals[h] for h in members], axis=0)
-        outs = [total[:, k * tok_rows : (k + 1) * tok_rows] for k in near]
-        backs.append(exchange(outs))
-    mixed = combine(share, backs)
+        return total
+
+    totals, turned = [], []
+    for h in range(PIECES):
+        sent, kept = down_product(ids, hidden, down_got[h])
+        came = swap(sent, "tp", 1)
+        if h < TP_FIRST:
+            totals.append(halve(add(kept, came)))
+        else:
+            cuts = weighted_cut(kept, came, share_all)
+            turned.append(add(*exchange(cuts)))
+    turned = jnp.concatenate([x.reshape(z_count, -1, tok_rows) for x in turned], axis=1)
+    ready = [
+        [turned[0]]
+        + [swap(turned[place_of(m, z_count)], "tp", 2 * m) for m in range(1, z_count)]
+    ]
+    total = jnp.concatenate(totals, axis=0)
+    outs = [total[:, k * tok_rows : (k + 1) * tok_rows] for k in near]
+    full = lay_pieces(ids, down_got)
+    mixed = combine(share, [exchange(outs)], ready)
 
     shape = (1, fs_count * gate_weight.shape[1], gate_weight.shape[2])
     return (mixed, gate_full.reshape(shape), up_full.reshape(shape), full.reshape(shape))

time: 174 us -> 159 us (0.914)
  waiting for transfers between devices: 94.7 us -> 66.9 us
  starting transfers between devices: 54.9 us -> 67.3 us
    ppermute x53 -> x58, waiting for transfers between devices: 94.7 us -> 66.9 us  [swap(): return lax.ppermute(x, axis, [(s, s ^ distance) for s in range(count)])]
    ppermute x53 -> x58, starting transfers between devices: 54.9 us -> 67.3 us  [swap(): return lax.ppermute(x, axis, [(s, s ^ distance) for s in range(count)])]
    pallas_call x11 -> x14, Pallas kernels: 19.5 us -> 19.8 us  [call(): pl.pallas_call(body, out_shape=outs, cost_estimate=pl.CostEstimate(flops=...]
  transfers between devices with their start and end apart: 53 -> 58, of which waited for: 22 -> 23; matrix products, arithmetic and copies ran while one was open for 1% -> 1% of each run, Pallas kernels for 10% -> 12%
where the time goes in v2:
time: 159 us
  starting transfers between devices  67.3 us (42%)
  waiting for transfers between devices  66.9 us (42%)
  Pallas kernels  19.8 us (12%)
  local copies, waits for them, and re-layouts  2.95 us (2%)
    ppermute x58, starting transfers between devices, swap(): return lax.ppermute(x, axis, [(s, s ^ distance) for s in range(count)])  67.3 us
    ppermute x58, waiting for transfers between devices, swap(): return lax.ppermute(x, axis, [(s, s ^ distance) for s in range(count)])  66.9 us
    pallas_call x14, Pallas kernels, call(): pl.pallas_call(body, out_shape=outs, cost_estimate=pl.CostEstimate(flops=...  19.8 us
  transfers between devices with their start and end apart: 58, of which 23 were waited for; matrix products, arithmetic and copies ran while one was open for 1% of the time, Pallas kernels for 12%

profile of v2, /device:TPU:0, one launch (start us, length us, event | category | flops | bytes accessed | tf_op | source)
XLA Modules:
  0.0 158.8 jit_solution(1223864333139865872)
XLA Ops:
  0.6 3.0 %collective-permute-start.7 = (bf16[256,256]{1,0:T(8,128)(2,1)}, bf16[256,256]{1,0:T(8,128)(2,1)S(1)}, u32[]{:S(2)}, u32[]{:S(2)}) collective-permute-start(bf16[256,256]{1,0:T(8,128)(2,1)} %refs_0_.3), channel_id=1, source_target_pairs={{0,8},{8,0},{16,24},{24,16},{1,9},{9,1},{17,25},{25,17},{2,10},{10... | collective-permute-start | bytes 393224 | tf_op jit(solution)/shard_map/ppermute | solution.py:92
  5.2 2.0 %collective-permute-start.1 = (bf16[256,256]{1,0:T(8,128)(2,1)}, bf16[256,256]{1,0:T(8,128)(2,1)S(1)}, u32[]{:S(2)}, u32[]{:S(2)}) collective-permute-start(bf16[256,256]{1,0:T(8,128)(2,1)} %refs_0_.3), channel_id=1, source_target_pairs={{0,2},{1,3},{2,0},{3,1},{4,6},{5,7},{6,4},{7,5},{8,10},{9,11},{10,... | collective-permute-start | bytes 393224 | tf_op jit(solution)/shard_map/ppermute | solution.py:92
  7.2 2.6 %collective-permute-start.3 = (bf16[256,256]{1,0:T(8,128)(2,1)}, bf16[256,256]{1,0:T(8,128)(2,1)S(1)}, u32[]{:S(2)}, u32[]{:S(2)}) collective-permute-start(bf16[256,256]{1,0:T(8,128)(2,1)} %refs_0_.3), channel_id=1, source_target_pairs={{0,4},{1,5},{2,6},{3,7},{4,0},{5,1},{6,2},{7,3},{8,12},{9,13},{10,... | collective-permute-start | bytes 393224 | tf_op jit(solution)/shard_map/ppermute | solution.py:92
  12.3 2.6 %collective-permute-start.13 = (bf16[768,256]{1,0:T(8,128)(2,1)S(1)}, bf16[768,256]{1,0:T(8,128)(2,1)S(1)}, u32[]{:S(2)}, u32[]{:S(2)}) collective-permute-start(bf16[768,256]{1,0:T(8,128)(2,1)S(1)} %shard_map.102.refs_8_), channel_id=1, source_target_pairs={{0,4},{1,5},{2,6},{3,7},{4,0},{5,1},{6,2},{7,3},{8,12},{9,13},{10,... | collective-permute-start | bytes 1179656 | tf_op jit(solution)/shard_map/ppermute | solution.py:92
  17.4 9.9 %collective-permute-done.5.refs_6_ = bf16[256,256]{1,0:T(8,128)(2,1)S(1)} collective-permute-done((bf16[256,256]{1,0:T(8,128)(2,1)S(1)}, bf16[256,256]{1,0:T(8,128)(2,1)S(1)}, u32[]{:S(2)}, u32[]{:S(2)}) %collective-permute-start.5) | collective-permute-done | bytes 131104 | tf_op jit(solution)/shard_map/ppermute | solution.py:92
  27.4 2.2 %copy-done = f32[4,512,512]{2,1,0:T(8,128)S(1)} copy-done((f32[4,512,512]{2,1,0:T(8,128)S(1)}, f32[4,512,512]{2,1,0:T(8,128)}, u32[]{:S(2)}) %copy-start) | copy-done | bytes 4194328
  34.7 2.5 %collective-permute-start.15 = (bf16[768,256]{1,0:T(8,128)(2,1)S(1)}, bf16[768,256]{1,0:T(8,128)(2,1)S(1)}, u32[]{:S(2)}, u32[]{:S(2)}) collective-permute-start(bf16[768,256]{1,0:T(8,128)(2,1)S(1)} %collective-permute-done.13.refs_12_), channel_id=1, source_target_pairs={{0,2},{1,3},{2,0},{3,1},{4,6},{5,7},{6,4},{7,5},{8,10},{9,11},{10,... | collective-permute-start | bytes 1179656 | tf_op jit(solution)/shard_map/ppermute | solution.py:92
  37.1 8.8 %collective-permute-done.17.refs_17_ = bf16[512,512]{1,0:T(8,128)(2,1)S(1)} collective-permute-done((bf16[512,512]{1,0:T(8,128)(2,1)S(1)}, bf16[512,512]{1,0:T(8,128)(2,1)S(1)}, u32[]{:S(2)}, u32[]{:S(2)}) %collective-permute-start.17) | collective-permute-done | bytes 524320 | tf_op jit(solution)/shard_map/ppermute | solution.py:92
  47.3 9.0 %collective-permute-done.18.refs_18_ = bf16[512,512]{1,0:T(8,128)(2,1)S(1)} collective-permute-done((bf16[512,512]{1,0:T(8,128)(2,1)S(1)}, bf16[512,512]{1,0:T(8,128)(2,1)S(1)}, u32[]{:S(2)}, u32[]{:S(2)}) %collective-permute-start.18) | collective-permute-done | bytes 524320 | tf_op jit(solution)/shard_map/ppermute | solution.py:92
  62.6 1.9 %collective-permute-start.30 = (bf16[2,48,512]{2,1,0:T(8,128)(2,1)S(1)}, bf16[2,48,512]{2,1,0:T(8,128)(2,1)S(1)}, u32[]{:S(2)}, u32[]{:S(2)}) collective-permute-start(bf16[2,48,512]{2,1,0:T(8,128)(2,1)S(1)} %get-tuple-element.68), channel_id=1, source_target_pairs={{0,16},{8,24},{16,0},{24,8},{1,17},{9,25},{17,1},{25,9},{2,18},{10... | collective-permute-start | bytes 294920 | tf_op jit(solution)/shard_map/ppermute | solution.py:92
  64.4 4.8 %shard_map.104 = (f32[1024,512]{1,0:T(8,128)S(1)}, bf16[2048,512]{1,0:T(8,128)(2,1)}, f32[1024,128]{1,0:T(8,128)S(1)}) custom-call(s32[3]{0:T(128)S(1)} %pad_add_fusion.ids_ref, bf16[256,256]{1,0:T(8,128)(2,1)S(1)} %copy-done.3, bf16[256,256]{1,0:T(8,128)(2,1)S(1)} %collective-permute-done.refs_1_, bf16[256,256]{1,0:T(8,128)(2,1)S(1)} %collective-permute-done.1.refs_2_, ...), custom_call_target="tpu_custom_call" | custom-call | flops 2147483648 | bytes 6291456 | tf_op jit(solution)/shard_map/pallas_call | solution.py:110
  71.1 3.2 %collective-permute-start.31 = (bf16[2,48,512]{2,1,0:T(8,128)(2,1)S(1)}, bf16[2,48,512]{2,1,0:T(8,128)(2,1)S(1)}, u32[]{:S(2)}, u32[]{:S(2)}) collective-permute-start(bf16[2,48,512]{2,1,0:T(8,128)(2,1)S(1)} %get-tuple-element.69), channel_id=1, source_target_pairs={{0,24},{8,16},{16,8},{24,0},{1,25},{9,17},{17,9},{25,1},{2,26},{10... | collective-permute-start | bytes 294920 | tf_op jit(solution)/shard_map/ppermute | solution.py:92
  74.2 13.5 %collective-permute-done.21.refs_18_ = bf16[512,512]{1,0:T(8,128)(2,1)S(1)} collective-permute-done((bf16[512,512]{1,0:T(8,128)(2,1)S(1)}, bf16[512,512]{1,0:T(8,128)(2,1)S(1)}, u32[]{:S(2)}, u32[]{:S(2)}) %collective-permute-start.21) | collective-permute-done | bytes 524320 | tf_op jit(solution)/shard_map/ppermute | solution.py:92
  90.1 4.4 %shard_map.106 = (bf16[512,1024]{1,0:T(8,128)(2,1)S(1)}, bf16[2048,512]{1,0:T(8,128)(2,1)}) custom-call(s32[3]{0:T(128)S(1)} %pad_add_fusion.ids_ref, f32[1024,512]{1,0:T(8,128)S(1)} %get-tuple-element.53.ga_ref, f32[1024,128]{1,0:T(8,128)S(1)} %get-tuple-element.54.ss_ref, bf16[256,256]{1,0:T(8,128)(2,1)S(1)} %copy-done.3, ...), custom_call_target="tpu_custom_call" | custom-call | flops 2147483648 | bytes 6291456 | tf_op jit(solution)/shard_map/pallas_call | solution.py:110
  96.9 2.0 %collective-permute-start.44 = (f32[1,256]{1,0:T(1,128)S(1)}, f32[1,256]{1,0:T(1,128)S(1)}, u32[]{:S(2)}, u32[]{:S(2)}) collective-permute-start(f32[1,256]{1,0:T(1,128)S(1)} %get-tuple-element.103), channel_id=1, source_target_pairs={{0,24},{8,16},{16,8},{24,0},{1,25},{9,17},{17,9},{25,1},{2,26},{10... | collective-permute-start | bytes 3080 | tf_op jit(solution)/shard_map/ppermute | solution.py:92
  98.8 2.6 %collective-permute-done.44 = f32[1,256]{1,0:T(1,128)S(1)} collective-permute-done((f32[1,256]{1,0:T(1,128)S(1)}, f32[1,256]{1,0:T(1,128)S(1)}, u32[]{:S(2)}, u32[]{:S(2)}) %collective-permute-start.44) | collective-permute-done | bytes 1056 | tf_op jit(solution)/shard_map/ppermute | solution.py:92
  102.6 2.3 %collective-permute-done.43 = f32[1,256]{1,0:T(1,128)S(1)} collective-permute-done((f32[1,256]{1,0:T(1,128)S(1)}, f32[1,256]{1,0:T(1,128)S(1)}, u32[]{:S(2)}, u32[]{:S(2)}) %collective-permute-start.43) | collective-permute-done | bytes 1056 | tf_op jit(solution)/shard_map/ppermute | solution.py:92
  117.1 2.3 %collective-permute-done.38.refs_1_.refs_9_ = bf16[2,80,512]{2,1,0:T(8,128)(2,1)S(1)} collective-permute-done((bf16[2,80,512]{2,1,0:T(8,128)(2,1)S(1)}, bf16[2,80,512]{2,1,0:T(8,128)(2,1)S(1)}, u32[]{:S(2)}, u32[]{:S(2)}) %collective-permute-start.38) | collective-permute-done | bytes 163872 | tf_op jit(solution)/shard_map/ppermute | solution.py:92
  119.4 2.7 %collective-permute-done.39.refs_2_.refs_10_ = bf16[2,80,512]{2,1,0:T(8,128)(2,1)S(1)} collective-permute-done((bf16[2,80,512]{2,1,0:T(8,128)(2,1)S(1)}, bf16[2,80,512]{2,1,0:T(8,128)(2,1)S(1)}, u32[]{:S(2)}, u32[]{:S(2)}) %collective-permute-start.39) | collective-permute-done | bytes 163872 | tf_op jit(solution)/shard_map/ppermute | solution.py:92
  125.1 2.5 %collective-permute-start.33 = (bf16[96,1024]{1,0:T(8,128)(2,1)S(1)}, bf16[96,1024]{1,0:T(8,128)(2,1)S(1)}, u32[]{:S(2)}, u32[]{:S(2)}) collective-permute-start(bf16[96,1024]{1,0:T(8,128)(2,1)S(1)} %slice.85), channel_id=1, source_target_pairs={{0,2},{1,3},{2,0},{3,1},{4,6},{5,7},{6,4},{7,5},{8,10},{9,11},{10,... | collective-permute-start | bytes 589832 | tf_op jit(solution)/shard_map/ppermute | solution.py:92
  130.5 2.9 %collective-permute-done.33 = bf16[96,1024]{1,0:T(8,128)(2,1)S(1)} collective-permute-done((bf16[96,1024]{1,0:T(8,128)(2,1)S(1)}, bf16[96,1024]{1,0:T(8,128)(2,1)S(1)}, u32[]{:S(2)}, u32[]{:S(2)}) %collective-permute-start.33) | collective-permute-done | bytes 196640 | tf_op jit(solution)/shard_map/ppermute | solution.py:92
  134.3 2.1 %collective-permute-start.34 = (bf16[48,1024]{1,0:T(8,128)(2,1)S(1)}, bf16[48,1024]{1,0:T(8,128)(2,1)S(1)}, u32[]{:S(2)}, u32[]{:S(2)}) collective-permute-start(bf16[48,1024]{1,0:T(8,128)(2,1)S(1)} %slice.87), channel_id=1, source_target_pairs={{0,4},{1,5},{2,6},{3,7},{4,0},{5,1},{6,2},{7,3},{8,12},{9,13},{10,... | collective-permute-start | bytes 294920 | tf_op jit(solution)/shard_map/ppermute | solution.py:92
  141.1 2.7 %collective-permute-start.28 = (bf16[64,1024]{1,0:T(8,128)(2,1)S(1)}, bf16[64,1024]{1,0:T(8,128)(2,1)S(1)}, u32[]{:S(2)}, u32[]{:S(2)}) collective-permute-start(bf16[64,1024]{1,0:T(8,128)(2,1)S(1)} %slice.83), channel_id=1, source_target_pairs={{0,4},{1,5},{2,6},{3,7},{4,0},{5,1},{6,2},{7,3},{8,12},{9,13},{10,... | collective-permute-start | bytes 393224 | tf_op jit(solution)/shard_map/ppermute | solution.py:92
  154.5 2.0 %shard_map.115 = bf16[4,2,256,512]{3,2,1,0:T(8,128)(2,1)} custom-call(s32[3]{0:T(128)S(1)} %pad_add_fusion.ids_ref, bf16[2,64,512]{2,1,0:T(8,128)(2,1)S(1)} %get-tuple-element.60.refs_0_, bf16[2,64,512]{2,1,0:T(8,128)(2,1)S(1)} %collective-permute-done.23.refs_1_, bf16[2,64,512]{2,1,0:T(8,128)(2,1)S(1)} %collective-permute-done.24.refs_2_, ...), custom_call_target="tpu_custom_call" | custom-call | bytes 4194304 | tf_op jit(solution)/shard_map/pallas_call | solution.py:110
  (139 shorter events, 63.4 us)
Async XLA Ops:
  11.7 21.8 %collective-permute-start.10 = (bf16[768,256]{1,0:T(8,128)(2,1)S(1)}, bf16[768,256]{1,0:T(8,128)(2,1)S(1)}, u32[]{:S(2)}, u32[]{:S(2)}) collective-permute-start(bf16[768,256]{1,0:T(8,128)(2,1)S(1)} %shard_map.102.refs_8_), channel_id=1, source_target_pairs={{0,1},{1,0},{2,3},{3,2},{4,5},{5,4},{6,7},{7,6},{8,9},{9,8},{10,11... | collective-permute-start | bytes 1179656 | tf_op jit(solution)/shard_map/ppermute | solution.py:92
  12.3 22.3 %collective-permute-start.13 = (bf16[768,256]{1,0:T(8,128)(2,1)S(1)}, bf16[768,256]{1,0:T(8,128)(2,1)S(1)}, u32[]{:S(2)}, u32[]{:S(2)}) collective-permute-start(bf16[768,256]{1,0:T(8,128)(2,1)S(1)} %shard_map.102.refs_8_), channel_id=1, source_target_pairs={{0,4},{1,5},{2,6},{3,7},{4,0},{5,1},{6,2},{7,3},{8,12},{9,13},{10,... | collective-permute-start | bytes 1179656 | tf_op jit(solution)/shard_map/ppermute | solution.py:92
  15.3 12.0 %collective-permute-start.5 = (bf16[256,256]{1,0:T(8,128)(2,1)S(1)}, bf16[256,256]{1,0:T(8,128)(2,1)S(1)}, u32[]{:S(2)}, u32[]{:S(2)}) collective-permute-start(bf16[256,256]{1,0:T(8,128)(2,1)S(1)} %collective-permute-done.3.refs_4_), channel_id=1, source_target_pairs={{0,2},{1,3},{2,0},{3,1},{4,6},{5,7},{6,4},{7,5},{8,10},{9,11},{10,... | collective-permute-start | bytes 393224 | tf_op jit(solution)/shard_map/ppermute | solution.py:92
  16.5 20.6 %collective-permute-start.11 = (bf16[768,256]{1,0:T(8,128)(2,1)S(1)}, bf16[768,256]{1,0:T(8,128)(2,1)S(1)}, u32[]{:S(2)}, u32[]{:S(2)}) collective-permute-start(bf16[768,256]{1,0:T(8,128)(2,1)S(1)} %shard_map.102.refs_8_), channel_id=1, source_target_pairs={{0,2},{1,3},{2,0},{3,1},{4,6},{5,7},{6,4},{7,5},{8,10},{9,11},{10,... | collective-permute-start | bytes 1179656 | tf_op jit(solution)/shard_map/ppermute | solution.py:92
  17.4 13.7 %collective-permute-start.4 = (bf16[256,256]{1,0:T(8,128)(2,1)S(1)}, bf16[256,256]{1,0:T(8,128)(2,1)S(1)}, u32[]{:S(2)}, u32[]{:S(2)}) collective-permute-start(bf16[256,256]{1,0:T(8,128)(2,1)S(1)} %collective-permute-done.3.refs_4_), channel_id=1, source_target_pairs={{0,1},{1,0},{2,3},{3,2},{4,5},{5,4},{6,7},{7,6},{8,9},{9,8},{10,11... | collective-permute-start | bytes 393224 | tf_op jit(solution)/shard_map/ppermute | solution.py:92
  31.1 14.9 %collective-permute-start.17 = (bf16[512,512]{1,0:T(8,128)(2,1)S(1)}, bf16[512,512]{1,0:T(8,128)(2,1)S(1)}, u32[]{:S(2)}, u32[]{:S(2)}) collective-permute-start(bf16[512,512]{1,0:T(8,128)(2,1)S(1)} %get-tuple-element.50), channel_id=1, source_target_pairs={{0,8},{8,0},{16,24},{24,16},{1,9},{9,1},{17,25},{25,17},{2,10},{10... | collective-permute-start | bytes 1572872 | tf_op jit(solution)/shard_map/ppermute | solution.py:92
  32.4 23.9 %collective-permute-start.18 = (bf16[512,512]{1,0:T(8,128)(2,1)S(1)}, bf16[512,512]{1,0:T(8,128)(2,1)S(1)}, u32[]{:S(2)}, u32[]{:S(2)}) collective-permute-start(bf16[512,512]{1,0:T(8,128)(2,1)S(1)} %get-tuple-element.51), channel_id=1, source_target_pairs={{0,16},{8,24},{16,0},{24,8},{1,17},{9,25},{17,1},{25,9},{2,18},{10... | collective-permute-start | bytes 1572872 | tf_op jit(solution)/shard_map/ppermute | solution.py:92
  33.5 24.6 %collective-permute-start.19 = (bf16[512,512]{1,0:T(8,128)(2,1)S(1)}, bf16[512,512]{1,0:T(8,128)(2,1)S(1)}, u32[]{:S(2)}, u32[]{:S(2)}) collective-permute-start(bf16[512,512]{1,0:T(8,128)(2,1)S(1)} %get-tuple-element.52), channel_id=1, source_target_pairs={{0,24},{8,16},{16,8},{24,0},{1,25},{9,17},{17,9},{25,1},{2,26},{10... | collective-permute-start | bytes 1572872 | tf_op jit(solution)/shard_map/ppermute | solution.py:92
  34.7 11.4 %collective-permute-start.15 = (bf16[768,256]{1,0:T(8,128)(2,1)S(1)}, bf16[768,256]{1,0:T(8,128)(2,1)S(1)}, u32[]{:S(2)}, u32[]{:S(2)}) collective-permute-start(bf16[768,256]{1,0:T(8,128)(2,1)S(1)} %collective-permute-done.13.refs_12_), channel_id=1, source_target_pairs={{0,2},{1,3},{2,0},{3,1},{4,6},{5,7},{6,4},{7,5},{8,10},{9,11},{10,... | collective-permute-start | bytes 1179656 | tf_op jit(solution)/shard_map/ppermute | solution.py:92
  37.1 22.8 %collective-permute-start.12 = (bf16[768,256]{1,0:T(8,128)(2,1)S(1)}, bf16[768,256]{1,0:T(8,128)(2,1)S(1)}, u32[]{:S(2)}, u32[]{:S(2)}) collective-permute-start(bf16[768,256]{1,0:T(8,128)(2,1)S(1)} %collective-permute-done.11.refs_10_), channel_id=1, source_target_pairs={{0,1},{1,0},{2,3},{3,2},{4,5},{5,4},{6,7},{7,6},{8,9},{9,8},{10,11... | collective-permute-start | bytes 1179656 | tf_op jit(solution)/shard_map/ppermute | solution.py:92
  45.9 15.4 %collective-permute-start.14 = (bf16[768,256]{1,0:T(8,128)(2,1)S(1)}, bf16[768,256]{1,0:T(8,128)(2,1)S(1)}, u32[]{:S(2)}, u32[]{:S(2)}) collective-permute-start(bf16[768,256]{1,0:T(8,128)(2,1)S(1)} %collective-permute-done.13.refs_12_), channel_id=1, source_target_pairs={{0,1},{1,0},{2,3},{3,2},{4,5},{5,4},{6,7},{7,6},{8,9},{9,8},{10,11... | collective-permute-start | bytes 1179656 | tf_op jit(solution)/shard_map/ppermute | solution.py:92
  46.1 16.5 %collective-permute-start.16 = (bf16[768,256]{1,0:T(8,128)(2,1)S(1)}, bf16[768,256]{1,0:T(8,128)(2,1)S(1)}, u32[]{:S(2)}, u32[]{:S(2)}) collective-permute-start(bf16[768,256]{1,0:T(8,128)(2,1)S(1)} %collective-permute-done.15.refs_14_), channel_id=1, source_target_pairs={{0,1},{1,0},{2,3},{3,2},{4,5},{5,4},{6,7},{7,6},{8,9},{9,8},{10,11... | collective-permute-start | bytes 1179656 | tf_op jit(solution)/shard_map/ppermute | solution.py:92
  56.3 14.8 %collective-permute-start.20 = (bf16[512,512]{1,0:T(8,128)(2,1)S(1)}, bf16[512,512]{1,0:T(8,128)(2,1)S(1)}, u32[]{:S(2)}, u32[]{:S(2)}) collective-permute-start(bf16[512,512]{1,0:T(8,128)(2,1)S(1)} %get-tuple-element.56), channel_id=1, source_target_pairs={{0,8},{8,0},{16,24},{24,16},{1,9},{9,1},{17,25},{25,17},{2,10},{10... | collective-permute-start | bytes 1572872 | tf_op jit(solution)/shard_map/ppermute | solution.py:92
  58.1 29.5 %collective-permute-start.21 = (bf16[512,512]{1,0:T(8,128)(2,1)S(1)}, bf16[512,512]{1,0:T(8,128)(2,1)S(1)}, u32[]{:S(2)}, u32[]{:S(2)}) collective-permute-start(bf16[512,512]{1,0:T(8,128)(2,1)S(1)} %get-tuple-element.57), channel_id=1, source_target_pairs={{0,16},{8,24},{16,0},{24,8},{1,17},{9,25},{17,1},{25,9},{2,18},{10... | collective-permute-start | bytes 1572872 | tf_op jit(solution)/shard_map/ppermute | solution.py:92
  60.0 28.5 %collective-permute-start.22 = (bf16[512,512]{1,0:T(8,128)(2,1)S(1)}, bf16[512,512]{1,0:T(8,128)(2,1)S(1)}, u32[]{:S(2)}, u32[]{:S(2)}) collective-permute-start(bf16[512,512]{1,0:T(8,128)(2,1)S(1)} %get-tuple-element.58), channel_id=1, source_target_pairs={{0,24},{8,16},{16,8},{24,0},{1,25},{9,17},{17,9},{25,1},{2,26},{10... | collective-permute-start | bytes 1572872 | tf_op jit(solution)/shard_map/ppermute | solution.py:92
  61.4 33.1 %collective-permute-start.29 = (bf16[2,48,512]{2,1,0:T(8,128)(2,1)S(1)}, bf16[2,48,512]{2,1,0:T(8,128)(2,1)S(1)}, u32[]{:S(2)}, u32[]{:S(2)}) collective-permute-start(bf16[2,48,512]{2,1,0:T(8,128)(2,1)S(1)} %get-tuple-element.67), channel_id=1, source_target_pairs={{0,8},{8,0},{16,24},{24,16},{1,9},{9,1},{17,25},{25,17},{2,10},{10... | collective-permute-start | bytes 294920 | tf_op jit(solution)/shard_map/ppermute | solution.py:92
  62.6 33.0 %collective-permute-start.30 = (bf16[2,48,512]{2,1,0:T(8,128)(2,1)S(1)}, bf16[2,48,512]{2,1,0:T(8,128)(2,1)S(1)}, u32[]{:S(2)}, u32[]{:S(2)}) collective-permute-start(bf16[2,48,512]{2,1,0:T(8,128)(2,1)S(1)} %get-tuple-element.68), channel_id=1, source_target_pairs={{0,16},{8,24},{16,0},{24,8},{1,17},{9,25},{17,1},{25,9},{2,18},{10... | collective-permute-start | bytes 294920 | tf_op jit(solution)/shard_map/ppermute | solution.py:92
  71.1 24.6 %collective-permute-start.31 = (bf16[2,48,512]{2,1,0:T(8,128)(2,1)S(1)}, bf16[2,48,512]{2,1,0:T(8,128)(2,1)S(1)}, u32[]{:S(2)}, u32[]{:S(2)}) collective-permute-start(bf16[2,48,512]{2,1,0:T(8,128)(2,1)S(1)} %get-tuple-element.69), channel_id=1, source_target_pairs={{0,24},{8,16},{16,8},{24,0},{1,25},{9,17},{17,9},{25,1},{2,26},{10... | collective-permute-start | bytes 294920 | tf_op jit(solution)/shard_map/ppermute | solution.py:92
  87.7 18.2 %collective-permute-start.23 = (bf16[2,64,512]{2,1,0:T(8,128)(2,1)S(1)}, bf16[2,64,512]{2,1,0:T(8,128)(2,1)S(1)}, u32[]{:S(2)}, u32[]{:S(2)}) collective-permute-start(bf16[2,64,512]{2,1,0:T(8,128)(2,1)S(1)} %get-tuple-element.61), channel_id=1, source_target_pairs={{0,8},{8,0},{16,24},{24,16},{1,9},{9,1},{17,25},{25,17},{2,10},{10... | collective-permute-start | bytes 393224 | tf_op jit(solution)/shard_map/ppermute | solution.py:92
  88.5 18.9 %collective-permute-start.24 = (bf16[2,64,512]{2,1,0:T(8,128)(2,1)S(1)}, bf16[2,64,512]{2,1,0:T(8,128)(2,1)S(1)}, u32[]{:S(2)}, u32[]{:S(2)}) collective-permute-start(bf16[2,64,512]{2,1,0:T(8,128)(2,1)S(1)} %get-tuple-element.62), channel_id=1, source_target_pairs={{0,16},{8,24},{16,0},{24,8},{1,17},{9,25},{17,1},{25,9},{2,18},{10... | collective-permute-start | bytes 393224 | tf_op jit(solution)/shard_map/ppermute | solution.py:92
  94.5 13.9 %collective-permute-start.25 = (bf16[2,64,512]{2,1,0:T(8,128)(2,1)S(1)}, bf16[2,64,512]{2,1,0:T(8,128)(2,1)S(1)}, u32[]{:S(2)}, u32[]{:S(2)}) collective-permute-start(bf16[2,64,512]{2,1,0:T(8,128)(2,1)S(1)} %get-tuple-element.63), channel_id=1, source_target_pairs={{0,24},{8,16},{16,8},{24,0},{1,25},{9,17},{17,9},{25,1},{2,26},{10... | collective-permute-start | bytes 393224 | tf_op jit(solution)/shard_map/ppermute | solution.py:92
  96.8 28.2 %collective-permute-start.32 = (bf16[192,1024]{1,0:T(8,128)(2,1)S(1)}, bf16[192,1024]{1,0:T(8,128)(2,1)S(1)}, u32[]{:S(2)}, u32[]{:S(2)}) collective-permute-start(bf16[192,1024]{1,0:T(8,128)(2,1)S(1)} %get-tuple-element.71), channel_id=1, source_target_pairs={{0,1},{1,0},{2,3},{3,2},{4,5},{5,4},{6,7},{7,6},{8,9},{9,8},{10,11... | collective-permute-start | bytes 1179656 | tf_op jit(solution)/shard_map/ppermute | solution.py:92
  112.3 15.4 %collective-permute-start.26 = (bf16[256,1024]{1,0:T(8,128)(2,1)S(1)}, bf16[256,1024]{1,0:T(8,128)(2,1)S(1)}, u32[]{:S(2)}, u32[]{:S(2)}) collective-permute-start(bf16[256,1024]{1,0:T(8,128)(2,1)S(1)} %get-tuple-element.65), channel_id=1, source_target_pairs={{0,1},{1,0},{2,3},{3,2},{4,5},{5,4},{6,7},{7,6},{8,9},{9,8},{10,11... | collective-permute-start | bytes 1572872 | tf_op jit(solution)/shard_map/ppermute | solution.py:92
  127.9 13.1 %collective-permute-start.27 = (bf16[128,1024]{1,0:T(8,128)(2,1)S(1)}, bf16[128,1024]{1,0:T(8,128)(2,1)S(1)}, u32[]{:S(2)}, u32[]{:S(2)}) collective-permute-start(bf16[128,1024]{1,0:T(8,128)(2,1)S(1)} %slice.81), channel_id=1, source_target_pairs={{0,2},{1,3},{2,0},{3,1},{4,6},{5,7},{6,4},{7,5},{8,10},{9,11},{10,... | collective-permute-start | bytes 786440 | tf_op jit(solution)/shard_map/ppermute | solution.py:92
  (41 other events, 290.8 us)

commit v3 on v2

--- a/solution.py
+++ b/solution.py
@@ -382,37 +382,58 @@
     )(kept, came, share)
 
 
-def combine(share, backs, ready):
-    count = len(backs[0])
-    rows = share.shape[1]
-    total_cols = sum(back[0].shape[0] for back in backs) + sum(terms[0].shape[0] for terms in ready)
+def weighted_halves(pairs, share):
+    count, cut = share.shape
+    cols = sum(pair[0].shape[0] for pair in pairs)
+    groups = sorted(range(count), key=lambda k: place_of(k, count))
 
     def kernel(share_ref, *refs):
+        kept_ref, sent_ref = refs[-2:]
+        first = 0
+        for one, two in zip(refs[:-2:2], refs[1:-2:2]):
+            at = slice(first, first + one.shape[0])
+            for n, k in enumerate(groups):
+                span = slice(k * cut, (k + 1) * cut)
+                total = one[:, span].astype(jnp.float32) + two[:, span].astype(jnp.float32)
+                ref, place = (kept_ref, n) if 2 * n < count else (sent_ref, n - count // 2)
+                value = (total * share_ref[k : k + 1, :]).astype(jnp.bfloat16)
+                ref[at, place * cut : (place + 1) * cut] = value
+            first += one.shape[0]
+
+    flat = [x for pair in pairs for x in pair]
+    return local_kernel(
+        kernel,
+        [jax.ShapeDtypeStruct((cols, count // 2 * cut), jnp.bfloat16)] * 2,
+        2 * cols * count * cut,
+        6 * cols * count * cut,
+        in_specs=[VMEM] * (1 + len(flat)),
+        out_specs=[VMEM] * 2,
+    )(share, *flat)
+
+
+def combine(ready):
+    rows = ready[0][0].shape[1]
+    total_cols = sum(terms[0].shape[0] for terms in ready)
+
+    def kernel(*refs):
         parts = []
-        for h in range(len(backs)):
-            total = 0.0
-            for k in range(count):
-                term = refs[h * count + k][...].astype(jnp.float32)
-                total = total + share_ref[k : k + 1, :] * term
-            parts.append(total)
-        rest = iter(refs[len(flat) : -1])
+        rest = iter(refs[:-1])
         for terms in ready:
             parts.append(sum(next(rest)[...].astype(jnp.float32) for _ in terms))
         refs[-1][...] = jnp.concatenate(parts, axis=0).T.astype(jnp.bfloat16)
 
-    flat = [x for back in backs for x in back]
     summed = [x for terms in ready for x in terms]
     return local_kernel(
         kernel,
         jax.ShapeDtypeStruct((rows, total_cols), jnp.bfloat16),
-        2 * rows * total_cols * count,
-        2 * rows * total_cols * count,
-        in_specs=[VMEM] * (1 + len(flat) + len(summed)),
+        2 * rows * total_cols * len(summed),
+        2 * rows * total_cols * len(summed),
+        in_specs=[VMEM] * len(summed),
         out_specs=VMEM,
-    )(share, *flat, *summed)
-
-
-SHARES = (4, 3, 5, 4)
+    )(*summed)
+
+
+SHARES = (4, 4, 4, 4)
 PIECES = len(SHARES)
 TILE = 256
 TP_FIRST = 2
@@ -460,13 +481,14 @@
     share_all = jnp.concatenate(shares, axis=0)
 
     def halve(total):
-        step = 1
+        step, came = 1, None
         while step < z_count:
+            if came is not None:
+                total = add(total, came)
             half = total.shape[0] // 2
             came = swap(total[half:], "tp", 2 * step)
-            total = add(total[:half], came)
-            step *= 2
-        return total
+            total, step = total[:half], 2 * step
+        return total, came
 
     totals, turned = [], []
     for h in range(PIECES):
@@ -478,14 +500,17 @@
             cuts = weighted_cut(kept, came, share_all)
             turned.append(add(*exchange(cuts)))
     turned = jnp.concatenate([x.reshape(z_count, -1, tok_rows) for x in turned], axis=1)
-    ready = [
-        [turned[0]]
-        + [swap(turned[place_of(m, z_count)], "tp", 2 * m) for m in range(1, z_count)]
-    ]
-    total = jnp.concatenate(totals, axis=0)
-    outs = [total[:, k * tok_rows : (k + 1) * tok_rows] for k in near]
+    last = [turned[0]]
+    last += [swap(turned[place_of(m, z_count)], "tp", 2 * m) for m in range(1, z_count)]
+    total, sent = weighted_halves(totals, share_all)
+    came, step = swap(sent, "fs", 1), 2
+    while step < fs_count:
+        total = add(total, came)
+        half = total.shape[1] // 2
+        came = swap(total[:, half:], "fs", step)
+        total, step = total[:, :half], 2 * step
     full = lay_pieces(ids, down_got)
-    mixed = combine(share, [exchange(outs)], ready)
+    mixed = combine([[total, came], last])
 
     shape = (1, fs_count * gate_weight.shape[1], gate_weight.shape[2])
     return (mixed, gate_full.reshape(shape), up_full.reshape(shape), full.reshape(shape))

time: 159 us -> 167 us (1.050)
  waiting for transfers between devices: 66.9 us -> 75.4 us
    ppermute x58 -> x57, waiting for transfers between devices: 66.9 us -> 75.4 us  [swap(): return lax.ppermute(x, axis, [(s, s ^ distance) for s in range(count)])]
    ppermute x58 -> x57, starting transfers between devices: 67.3 us -> 67.1 us  [swap(): return lax.ppermute(x, axis, [(s, s ^ distance) for s in range(count)])]
    pallas_call x14 -> x15, Pallas kernels: 19.8 us -> 19.8 us  [call(): pl.pallas_call(body, out_shape=outs, cost_estimate=pl.CostEstimate(flops=...]
  transfers between devices with their start and end apart: 58 -> 57, of which waited for: 23 -> 21; matrix products, arithmetic and copies ran while one was open for 1% -> 1% of each run, Pallas kernels for 12% -> 11%
where the time goes in v3:
time: 167 us
  waiting for transfers between devices  75.4 us (45%)
  starting transfers between devices  67.1 us (40%)
  Pallas kernels  19.8 us (12%)
  local copies, waits for them, and re-layouts  2.98 us (2%)
    ppermute x57, waiting for transfers between devices, swap(): return lax.ppermute(x, axis, [(s, s ^ distance) for s in range(count)])  75.4 us
    ppermute x57, starting transfers between devices, swap(): return lax.ppermute(x, axis, [(s, s ^ distance) for s in range(count)])  67.1 us
    pallas_call x15, Pallas kernels, call(): pl.pallas_call(body, out_shape=outs, cost_estimate=pl.CostEstimate(flops=...  19.8 us
  transfers between devices with their start and end apart: 57, of which 21 were waited for; matrix products, arithmetic and copies ran while one was open for 1% of the time, Pallas kernels for 11%

profile of v3, /device:TPU:0, one launch (start us, length us, event | category | flops | bytes accessed | tf_op | source)
XLA Modules:
  0.0 167.2 jit_solution(17688354697945463310)
XLA Ops:
  0.6 3.0 %collective-permute-start.10 = (bf16[256,256]{1,0:T(8,128)(2,1)}, bf16[256,256]{1,0:T(8,128)(2,1)S(1)}, u32[]{:S(2)}, u32[]{:S(2)}) collective-permute-start(bf16[256,256]{1,0:T(8,128)(2,1)} %refs_0_.3), channel_id=1, source_target_pairs={{0,8},{8,0},{16,24},{24,16},{1,9},{9,1},{17,25},{25,17},{2,10},{10... | collective-permute-start | bytes 393224 | tf_op jit(solution)/shard_map/ppermute | solution.py:92
  5.2 2.0 %collective-permute-start.4 = (bf16[256,256]{1,0:T(8,128)(2,1)}, bf16[256,256]{1,0:T(8,128)(2,1)S(1)}, u32[]{:S(2)}, u32[]{:S(2)}) collective-permute-start(bf16[256,256]{1,0:T(8,128)(2,1)} %refs_0_.3), channel_id=1, source_target_pairs={{0,2},{1,3},{2,0},{3,1},{4,6},{5,7},{6,4},{7,5},{8,10},{9,11},{10,... | collective-permute-start | bytes 393224 | tf_op jit(solution)/shard_map/ppermute | solution.py:92
  7.2 2.6 %collective-permute-start.6 = (bf16[256,256]{1,0:T(8,128)(2,1)}, bf16[256,256]{1,0:T(8,128)(2,1)S(1)}, u32[]{:S(2)}, u32[]{:S(2)}) collective-permute-start(bf16[256,256]{1,0:T(8,128)(2,1)} %refs_0_.3), channel_id=1, source_target_pairs={{0,4},{1,5},{2,6},{3,7},{4,0},{5,1},{6,2},{7,3},{8,12},{9,13},{10,... | collective-permute-start | bytes 393224 | tf_op jit(solution)/shard_map/ppermute | solution.py:92
  12.3 2.6 %collective-permute-start.16 = (bf16[768,256]{1,0:T(8,128)(2,1)S(1)}, bf16[768,256]{1,0:T(8,128)(2,1)S(1)}, u32[]{:S(2)}, u32[]{:S(2)}) collective-permute-start(bf16[768,256]{1,0:T(8,128)(2,1)S(1)} %shard_map.102.refs_8_), channel_id=1, source_target_pairs={{0,4},{1,5},{2,6},{3,7},{4,0},{5,1},{6,2},{7,3},{8,12},{9,13},{10,... | collective-permute-start | bytes 1179656 | tf_op jit(solution)/shard_map/ppermute | solution.py:92
  17.4 9.9 %collective-permute-done.8.refs_6_ = bf16[256,256]{1,0:T(8,128)(2,1)S(1)} collective-permute-done((bf16[256,256]{1,0:T(8,128)(2,1)S(1)}, bf16[256,256]{1,0:T(8,128)(2,1)S(1)}, u32[]{:S(2)}, u32[]{:S(2)}) %collective-permute-start.8) | collective-permute-done | bytes 131104 | tf_op jit(solution)/shard_map/ppermute | solution.py:92
  27.4 2.2 %copy-done = f32[4,512,512]{2,1,0:T(8,128)S(1)} copy-done((f32[4,512,512]{2,1,0:T(8,128)S(1)}, f32[4,512,512]{2,1,0:T(8,128)}, u32[]{:S(2)}) %copy-start) | copy-done | bytes 4194328
  34.7 2.5 %collective-permute-start.18 = (bf16[768,256]{1,0:T(8,128)(2,1)S(1)}, bf16[768,256]{1,0:T(8,128)(2,1)S(1)}, u32[]{:S(2)}, u32[]{:S(2)}) collective-permute-start(bf16[768,256]{1,0:T(8,128)(2,1)S(1)} %collective-permute-done.16.refs_12_), channel_id=1, source_target_pairs={{0,2},{1,3},{2,0},{3,1},{4,6},{5,7},{6,4},{7,5},{8,10},{9,11},{10,... | collective-permute-start | bytes 1179656 | tf_op jit(solution)/shard_map/ppermute | solution.py:92
  37.1 8.8 %collective-permute-done.20.refs_17_ = bf16[512,512]{1,0:T(8,128)(2,1)S(1)} collective-permute-done((bf16[512,512]{1,0:T(8,128)(2,1)S(1)}, bf16[512,512]{1,0:T(8,128)(2,1)S(1)}, u32[]{:S(2)}, u32[]{:S(2)}) %collective-permute-start.20) | collective-permute-done | bytes 524320 | tf_op jit(solution)/shard_map/ppermute | solution.py:92
  47.3 9.0 %collective-permute-done.21.refs_18_ = bf16[512,512]{1,0:T(8,128)(2,1)S(1)} collective-permute-done((bf16[512,512]{1,0:T(8,128)(2,1)S(1)}, bf16[512,512]{1,0:T(8,128)(2,1)S(1)}, u32[]{:S(2)}, u32[]{:S(2)}) %collective-permute-start.21) | collective-permute-done | bytes 524320 | tf_op jit(solution)/shard_map/ppermute | solution.py:92
  64.4 4.8 %shard_map.104 = (f32[1024,512]{1,0:T(8,128)S(1)}, bf16[2048,512]{1,0:T(8,128)(2,1)}, f32[1024,128]{1,0:T(8,128)S(1)}) custom-call(s32[3]{0:T(128)S(1)} %pad_add_fusion.ids_ref, bf16[256,256]{1,0:T(8,128)(2,1)S(1)} %copy-done.3, bf16[256,256]{1,0:T(8,128)(2,1)S(1)} %collective-permute-done.3.refs_1_, bf16[256,256]{1,0:T(8,128)(2,1)S(1)} %collective-permute-done.4.refs_2_, ...), custom_call_target="tpu_custom_call" | custom-call | flops 2147483648 | bytes 6291456 | tf_op jit(solution)/shard_map/pallas_call | solution.py:110
  71.1 3.2 %collective-permute-start.28 = (bf16[2,64,512]{2,1,0:T(8,128)(2,1)S(1)}, bf16[2,64,512]{2,1,0:T(8,128)(2,1)S(1)}, u32[]{:S(2)}, u32[]{:S(2)}) collective-permute-start(bf16[2,64,512]{2,1,0:T(8,128)(2,1)S(1)} %get-tuple-element.65), channel_id=1, source_target_pairs={{0,24},{8,16},{16,8},{24,0},{1,25},{9,17},{17,9},{25,1},{2,26},{10... | collective-permute-start | bytes 393224 | tf_op jit(solution)/shard_map/ppermute | solution.py:92
  74.2 13.3 %collective-permute-done.24.refs_18_ = bf16[512,512]{1,0:T(8,128)(2,1)S(1)} collective-permute-done((bf16[512,512]{1,0:T(8,128)(2,1)S(1)}, bf16[512,512]{1,0:T(8,128)(2,1)S(1)}, u32[]{:S(2)}, u32[]{:S(2)}) %collective-permute-start.24) | collective-permute-done | bytes 524320 | tf_op jit(solution)/shard_map/ppermute | solution.py:92
  88.4 2.6 %collective-permute-start.33 = (bf16[2,64,512]{2,1,0:T(8,128)(2,1)S(1)}, bf16[2,64,512]{2,1,0:T(8,128)(2,1)S(1)}, u32[]{:S(2)}, u32[]{:S(2)}) collective-permute-start(bf16[2,64,512]{2,1,0:T(8,128)(2,1)S(1)} %get-tuple-element.70), channel_id=1, source_target_pairs={{0,16},{8,24},{16,0},{24,8},{1,17},{9,25},{17,1},{25,9},{2,18},{10... | collective-permute-start | bytes 393224 | tf_op jit(solution)/shard_map/ppermute | solution.py:92
  91.1 4.4 %shard_map.106 = (bf16[512,1024]{1,0:T(8,128)(2,1)S(1)}, bf16[2048,512]{1,0:T(8,128)(2,1)}) custom-call(s32[3]{0:T(128)S(1)} %pad_add_fusion.ids_ref, f32[1024,512]{1,0:T(8,128)S(1)} %get-tuple-element.55.ga_ref, f32[1024,128]{1,0:T(8,128)S(1)} %get-tuple-element.56.ss_ref, bf16[256,256]{1,0:T(8,128)(2,1)S(1)} %copy-done.3, ...), custom_call_target="tpu_custom_call" | custom-call | flops 2147483648 | bytes 6291456 | tf_op jit(solution)/shard_map/pallas_call | solution.py:110
  97.3 2.6 %collective-permute-start.2 = (f32[1,256]{1,0:T(1,128)S(1)}, f32[1,256]{1,0:T(1,128)S(1)}, u32[]{:S(2)}, u32[]{:S(2)}) collective-permute-start(f32[1,256]{1,0:T(1,128)S(1)} %get-tuple-element.109), channel_id=1, source_target_pairs={{0,24},{8,16},{16,8},{24,0},{1,25},{9,17},{17,9},{25,1},{2,26},{10... | collective-permute-start | bytes 3080 | tf_op jit(solution)/shard_map/ppermute | solution.py:92
  101.8 2.0 %collective-permute-start.1 = (f32[1,256]{1,0:T(1,128)S(1)}, f32[1,256]{1,0:T(1,128)S(1)}, u32[]{:S(2)}, u32[]{:S(2)}) collective-permute-start(f32[1,256]{1,0:T(1,128)S(1)} %get-tuple-element.110), channel_id=1, source_target_pairs={{0,16},{8,24},{16,0},{24,8},{1,17},{9,25},{17,1},{25,9},{2,18},{10... | collective-permute-start | bytes 3080 | tf_op jit(solution)/shard_map/ppermute | solution.py:92
  106.5 2.0 %collective-permute-start.48 = (bf16[2,64,512]{2,1,0:T(8,128)(2,1)S(1)}, bf16[2,64,512]{2,1,0:T(8,128)(2,1)S(1)}, u32[]{:S(2)}, u32[]{:S(2)}) collective-permute-start(bf16[2,64,512]{2,1,0:T(8,128)(2,1)S(1)} %get-tuple-element.88), channel_id=1, source_target_pairs={{0,16},{8,24},{16,0},{24,8},{1,17},{9,25},{17,1},{25,9},{2,18},{10... | collective-permute-start | bytes 393224 | tf_op jit(solution)/shard_map/ppermute | solution.py:92
  119.4 2.4 %collective-permute-done.41.refs_2_.refs_10_ = bf16[2,64,512]{2,1,0:T(8,128)(2,1)S(1)} collective-permute-done((bf16[2,64,512]{2,1,0:T(8,128)(2,1)S(1)}, bf16[2,64,512]{2,1,0:T(8,128)(2,1)S(1)}, u32[]{:S(2)}, u32[]{:S(2)}) %collective-permute-start.41) | collective-permute-done | bytes 131104 | tf_op jit(solution)/shard_map/ppermute | solution.py:92
  124.7 2.5 %collective-permute-start.30 = (bf16[128,1024]{1,0:T(8,128)(2,1)S(1)}, bf16[128,1024]{1,0:T(8,128)(2,1)S(1)}, u32[]{:S(2)}, u32[]{:S(2)}) collective-permute-start(bf16[128,1024]{1,0:T(8,128)(2,1)S(1)} %slice.77), channel_id=1, source_target_pairs={{0,2},{1,3},{2,0},{3,1},{4,6},{5,7},{6,4},{7,5},{8,10},{9,11},{10,... | collective-permute-start | bytes 786440 | tf_op jit(solution)/shard_map/ppermute | solution.py:92
  131.5 3.0 %collective-permute-done.30 = bf16[128,1024]{1,0:T(8,128)(2,1)S(1)} collective-permute-done((bf16[128,1024]{1,0:T(8,128)(2,1)S(1)}, bf16[128,1024]{1,0:T(8,128)(2,1)S(1)}, u32[]{:S(2)}, u32[]{:S(2)}) %collective-permute-start.30) | collective-permute-done | bytes 262176 | tf_op jit(solution)/shard_map/ppermute | solution.py:92
  136.3 3.6 %collective-permute-done.36 = bf16[128,1024]{1,0:T(8,128)(2,1)S(1)} collective-permute-done((bf16[128,1024]{1,0:T(8,128)(2,1)S(1)}, bf16[128,1024]{1,0:T(8,128)(2,1)S(1)}, u32[]{:S(2)}, u32[]{:S(2)}) %collective-permute-start.36) | collective-permute-done | bytes 262176 | tf_op jit(solution)/shard_map/ppermute | solution.py:92
  145.3 9.3 %collective-permute-done.31.refs_1_ = bf16[64,1024]{1,0:T(8,128)(2,1)S(1)} collective-permute-done((bf16[64,1024]{1,0:T(8,128)(2,1)S(1)}, bf16[64,1024]{1,0:T(8,128)(2,1)S(1)}, u32[]{:S(2)}, u32[]{:S(2)}) %collective-permute-start.31) | collective-permute-done | bytes 131104 | tf_op jit(solution)/shard_map/ppermute | solution.py:92
  159.6 2.5 %collective-permute-start.56 = (bf16[128,256]{1,0:T(8,128)(2,1)S(1)}, bf16[128,256]{1,0:T(8,128)(2,1)S(1)}, u32[]{:S(2)}, u32[]{:S(2)}) collective-permute-start(bf16[128,256]{1,0:T(8,128)(2,1)S(1)} %get-tuple-element.98), channel_id=1, source_target_pairs={{0,6},{1,7},{2,4},{3,5},{4,2},{5,3},{6,0},{7,1},{8,14},{9,15},{10,... | collective-permute-start | bytes 196616 | tf_op jit(solution)/shard_map/ppermute | solution.py:92
  163.0 2.0 %shard_map.116 = bf16[4,2,256,512]{3,2,1,0:T(8,128)(2,1)} custom-call(s32[3]{0:T(128)S(1)} %pad_add_fusion.ids_ref, bf16[2,64,512]{2,1,0:T(8,128)(2,1)S(1)} %get-tuple-element.62.refs_0_, bf16[2,64,512]{2,1,0:T(8,128)(2,1)S(1)} %collective-permute-done.26.refs_1_, bf16[2,64,512]{2,1,0:T(8,128)(2,1)S(1)} %collective-permute-done.27.refs_2_, ...), custom_call_target="tpu_custom_call" | custom-call | bytes 4194304 | tf_op jit(solution)/shard_map/pallas_call | solution.py:110
  (137 shorter events, 63.6 us)
Async XLA Ops:
  11.7 21.8 %collective-permute-start.13 = (bf16[768,256]{1,0:T(8,128)(2,1)S(1)}, bf16[768,256]{1,0:T(8,128)(2,1)S(1)}, u32[]{:S(2)}, u32[]{:S(2)}) collective-permute-start(bf16[768,256]{1,0:T(8,128)(2,1)S(1)} %shard_map.102.refs_8_), channel_id=1, source_target_pairs={{0,1},{1,0},{2,3},{3,2},{4,5},{5,4},{6,7},{7,6},{8,9},{9,8},{10,11... | collective-permute-start | bytes 1179656 | tf_op jit(solution)/shard_map/ppermute | solution.py:92
  12.3 22.3 %collective-permute-start.16 = (bf16[768,256]{1,0:T(8,128)(2,1)S(1)}, bf16[768,256]{1,0:T(8,128)(2,1)S(1)}, u32[]{:S(2)}, u32[]{:S(2)}) collective-permute-start(bf16[768,256]{1,0:T(8,128)(2,1)S(1)} %shard_map.102.refs_8_), channel_id=1, source_target_pairs={{0,4},{1,5},{2,6},{3,7},{4,0},{5,1},{6,2},{7,3},{8,12},{9,13},{10,... | collective-permute-start | bytes 1179656 | tf_op jit(solution)/shard_map/ppermute | solution.py:92
  16.5 20.6 %collective-permute-start.14 = (bf16[768,256]{1,0:T(8,128)(2,1)S(1)}, bf16[768,256]{1,0:T(8,128)(2,1)S(1)}, u32[]{:S(2)}, u32[]{:S(2)}) collective-permute-start(bf16[768,256]{1,0:T(8,128)(2,1)S(1)} %shard_map.102.refs_8_), channel_id=1, source_target_pairs={{0,2},{1,3},{2,0},{3,1},{4,6},{5,7},{6,4},{7,5},{8,10},{9,11},{10,... | collective-permute-start | bytes 1179656 | tf_op jit(solution)/shard_map/ppermute | solution.py:92
  17.4 13.7 %collective-permute-start.7 = (bf16[256,256]{1,0:T(8,128)(2,1)S(1)}, bf16[256,256]{1,0:T(8,128)(2,1)S(1)}, u32[]{:S(2)}, u32[]{:S(2)}) collective-permute-start(bf16[256,256]{1,0:T(8,128)(2,1)S(1)} %collective-permute-done.6.refs_4_), channel_id=1, source_target_pairs={{0,1},{1,0},{2,3},{3,2},{4,5},{5,4},{6,7},{7,6},{8,9},{9,8},{10,11... | collective-permute-start | bytes 393224 | tf_op jit(solution)/shard_map/ppermute | solution.py:92
  31.1 14.9 %collective-permute-start.20 = (bf16[512,512]{1,0:T(8,128)(2,1)S(1)}, bf16[512,512]{1,0:T(8,128)(2,1)S(1)}, u32[]{:S(2)}, u32[]{:S(2)}) collective-permute-start(bf16[512,512]{1,0:T(8,128)(2,1)S(1)} %get-tuple-element.52), channel_id=1, source_target_pairs={{0,8},{8,0},{16,24},{24,16},{1,9},{9,1},{17,25},{25,17},{2,10},{10... | collective-permute-start | bytes 1572872 | tf_op jit(solution)/shard_map/ppermute | solution.py:92
  32.4 23.9 %collective-permute-start.21 = (bf16[512,512]{1,0:T(8,128)(2,1)S(1)}, bf16[512,512]{1,0:T(8,128)(2,1)S(1)}, u32[]{:S(2)}, u32[]{:S(2)}) collective-permute-start(bf16[512,512]{1,0:T(8,128)(2,1)S(1)} %get-tuple-element.53), channel_id=1, source_target_pairs={{0,16},{8,24},{16,0},{24,8},{1,17},{9,25},{17,1},{25,9},{2,18},{10... | collective-permute-start | bytes 1572872 | tf_op jit(solution)/shard_map/ppermute | solution.py:92
  33.5 24.6 %collective-permute-start.22 = (bf16[512,512]{1,0:T(8,128)(2,1)S(1)}, bf16[512,512]{1,0:T(8,128)(2,1)S(1)}, u32[]{:S(2)}, u32[]{:S(2)}) collective-permute-start(bf16[512,512]{1,0:T(8,128)(2,1)S(1)} %get-tuple-element.54), channel_id=1, source_target_pairs={{0,24},{8,16},{16,8},{24,0},{1,25},{9,17},{17,9},{25,1},{2,26},{10... | collective-permute-start | bytes 1572872 | tf_op jit(solution)/shard_map/ppermute | solution.py:92
  37.1 22.8 %collective-permute-start.15 = (bf16[768,256]{1,0:T(8,128)(2,1)S(1)}, bf16[768,256]{1,0:T(8,128)(2,1)S(1)}, u32[]{:S(2)}, u32[]{:S(2)}) collective-permute-start(bf16[768,256]{1,0:T(8,128)(2,1)S(1)} %collective-permute-done.14.refs_10_), channel_id=1, source_target_pairs={{0,1},{1,0},{2,3},{3,2},{4,5},{5,4},{6,7},{7,6},{8,9},{9,8},{10,11... | collective-permute-start | bytes 1179656 | tf_op jit(solution)/shard_map/ppermute | solution.py:92
  45.9 15.4 %collective-permute-start.17 = (bf16[768,256]{1,0:T(8,128)(2,1)S(1)}, bf16[768,256]{1,0:T(8,128)(2,1)S(1)}, u32[]{:S(2)}, u32[]{:S(2)}) collective-permute-start(bf16[768,256]{1,0:T(8,128)(2,1)S(1)} %collective-permute-done.16.refs_12_), channel_id=1, source_target_pairs={{0,1},{1,0},{2,3},{3,2},{4,5},{5,4},{6,7},{7,6},{8,9},{9,8},{10,11... | collective-permute-start | bytes 1179656 | tf_op jit(solution)/shard_map/ppermute | solution.py:92
  46.1 16.5 %collective-permute-start.19 = (bf16[768,256]{1,0:T(8,128)(2,1)S(1)}, bf16[768,256]{1,0:T(8,128)(2,1)S(1)}, u32[]{:S(2)}, u32[]{:S(2)}) collective-permute-start(bf16[768,256]{1,0:T(8,128)(2,1)S(1)} %collective-permute-done.18.refs_14_), channel_id=1, source_target_pairs={{0,1},{1,0},{2,3},{3,2},{4,5},{5,4},{6,7},{7,6},{8,9},{9,8},{10,11... | collective-permute-start | bytes 1179656 | tf_op jit(solution)/shard_map/ppermute | solution.py:92
  56.3 14.8 %collective-permute-start.23 = (bf16[512,512]{1,0:T(8,128)(2,1)S(1)}, bf16[512,512]{1,0:T(8,128)(2,1)S(1)}, u32[]{:S(2)}, u32[]{:S(2)}) collective-permute-start(bf16[512,512]{1,0:T(8,128)(2,1)S(1)} %get-tuple-element.58), channel_id=1, source_target_pairs={{0,8},{8,0},{16,24},{24,16},{1,9},{9,1},{17,25},{25,17},{2,10},{10... | collective-permute-start | bytes 1572872 | tf_op jit(solution)/shard_map/ppermute | solution.py:92
  58.1 29.4 %collective-permute-start.24 = (bf16[512,512]{1,0:T(8,128)(2,1)S(1)}, bf16[512,512]{1,0:T(8,128)(2,1)S(1)}, u32[]{:S(2)}, u32[]{:S(2)}) collective-permute-start(bf16[512,512]{1,0:T(8,128)(2,1)S(1)} %get-tuple-element.59), channel_id=1, source_target_pairs={{0,16},{8,24},{16,0},{24,8},{1,17},{9,25},{17,1},{25,9},{2,18},{10... | collective-permute-start | bytes 1572872 | tf_op jit(solution)/shard_map/ppermute | solution.py:92
  60.0 28.4 %collective-permute-start.25 = (bf16[512,512]{1,0:T(8,128)(2,1)S(1)}, bf16[512,512]{1,0:T(8,128)(2,1)S(1)}, u32[]{:S(2)}, u32[]{:S(2)}) collective-permute-start(bf16[512,512]{1,0:T(8,128)(2,1)S(1)} %get-tuple-element.60), channel_id=1, source_target_pairs={{0,24},{8,16},{16,8},{24,0},{1,25},{9,17},{17,9},{25,1},{2,26},{10... | collective-permute-start | bytes 1572872 | tf_op jit(solution)/shard_map/ppermute | solution.py:92
  61.4 34.1 %collective-permute-start.26 = (bf16[2,64,512]{2,1,0:T(8,128)(2,1)S(1)}, bf16[2,64,512]{2,1,0:T(8,128)(2,1)S(1)}, u32[]{:S(2)}, u32[]{:S(2)}) collective-permute-start(bf16[2,64,512]{2,1,0:T(8,128)(2,1)S(1)} %get-tuple-element.63), channel_id=1, source_target_pairs={{0,8},{8,0},{16,24},{24,16},{1,9},{9,1},{17,25},{25,17},{2,10},{10... | collective-permute-start | bytes 393224 | tf_op jit(solution)/shard_map/ppermute | solution.py:92
  62.6 33.3 %collective-permute-start.27 = (bf16[2,64,512]{2,1,0:T(8,128)(2,1)S(1)}, bf16[2,64,512]{2,1,0:T(8,128)(2,1)S(1)}, u32[]{:S(2)}, u32[]{:S(2)}) collective-permute-start(bf16[2,64,512]{2,1,0:T(8,128)(2,1)S(1)} %get-tuple-element.64), channel_id=1, source_target_pairs={{0,16},{8,24},{16,0},{24,8},{1,17},{9,25},{17,1},{25,9},{2,18},{10... | collective-permute-start | bytes 393224 | tf_op jit(solution)/shard_map/ppermute | solution.py:92
  71.1 24.8 %collective-permute-start.28 = (bf16[2,64,512]{2,1,0:T(8,128)(2,1)S(1)}, bf16[2,64,512]{2,1,0:T(8,128)(2,1)S(1)}, u32[]{:S(2)}, u32[]{:S(2)}) collective-permute-start(bf16[2,64,512]{2,1,0:T(8,128)(2,1)S(1)} %get-tuple-element.65), channel_id=1, source_target_pairs={{0,24},{8,16},{16,8},{24,0},{1,25},{9,17},{17,9},{25,1},{2,26},{10... | collective-permute-start | bytes 393224 | tf_op jit(solution)/shard_map/ppermute | solution.py:92
  87.5 19.0 %collective-permute-start.32 = (bf16[2,64,512]{2,1,0:T(8,128)(2,1)S(1)}, bf16[2,64,512]{2,1,0:T(8,128)(2,1)S(1)}, u32[]{:S(2)}, u32[]{:S(2)}) collective-permute-start(bf16[2,64,512]{2,1,0:T(8,128)(2,1)S(1)} %get-tuple-element.69), channel_id=1, source_target_pairs={{0,8},{8,0},{16,24},{24,16},{1,9},{9,1},{17,25},{25,17},{2,10},{10... | collective-permute-start | bytes 393224 | tf_op jit(solution)/shard_map/ppermute | solution.py:92
  88.4 20.1 %collective-permute-start.33 = (bf16[2,64,512]{2,1,0:T(8,128)(2,1)S(1)}, bf16[2,64,512]{2,1,0:T(8,128)(2,1)S(1)}, u32[]{:S(2)}, u32[]{:S(2)}) collective-permute-start(bf16[2,64,512]{2,1,0:T(8,128)(2,1)S(1)} %get-tuple-element.70), channel_id=1, source_target_pairs={{0,16},{8,24},{16,0},{24,8},{1,17},{9,25},{17,1},{25,9},{2,18},{10... | collective-permute-start | bytes 393224 | tf_op jit(solution)/shard_map/ppermute | solution.py:92
  97.2 27.3 %collective-permute-start.29 = (bf16[256,1024]{1,0:T(8,128)(2,1)S(1)}, bf16[256,1024]{1,0:T(8,128)(2,1)S(1)}, u32[]{:S(2)}, u32[]{:S(2)}) collective-permute-start(bf16[256,1024]{1,0:T(8,128)(2,1)S(1)} %get-tuple-element.67), channel_id=1, source_target_pairs={{0,1},{1,0},{2,3},{3,2},{4,5},{5,4},{6,7},{7,6},{8,9},{9,8},{10,11... | collective-permute-start | bytes 1572872 | tf_op jit(solution)/shard_map/ppermute | solution.py:92
  113.0 14.2 %collective-permute-start.35 = (bf16[256,1024]{1,0:T(8,128)(2,1)S(1)}, bf16[256,1024]{1,0:T(8,128)(2,1)S(1)}, u32[]{:S(2)}, u32[]{:S(2)}) collective-permute-start(bf16[256,1024]{1,0:T(8,128)(2,1)S(1)} %get-tuple-element.73), channel_id=1, source_target_pairs={{0,1},{1,0},{2,3},{3,2},{4,5},{5,4},{6,7},{7,6},{8,9},{9,8},{10,11... | collective-permute-start | bytes 1572872 | tf_op jit(solution)/shard_map/ppermute | solution.py:92
  130.2 13.9 %collective-permute-start.51 = (bf16[256,256]{1,0:T(8,128)(2,1)S(1)}, bf16[256,256]{1,0:T(8,128)(2,1)S(1)}, u32[]{:S(2)}, u32[]{:S(2)}) collective-permute-start(bf16[256,256]{1,0:T(8,128)(2,1)S(1)} %get-tuple-element.93), channel_id=1, source_target_pairs={{0,8},{8,0},{16,24},{24,16},{1,9},{9,1},{17,25},{25,17},{2,10},{10... | collective-permute-start | bytes 393224 | tf_op jit(solution)/shard_map/ppermute | solution.py:92
  134.4 23.1 %collective-permute-start.46 = (bf16[256,256]{1,0:T(8,128)(2,1)S(1)}, bf16[256,256]{1,0:T(8,128)(2,1)S(1)}, u32[]{:S(2)}, u32[]{:S(2)}) collective-permute-start(bf16[256,256]{1,0:T(8,128)(2,1)S(1)} %get-tuple-element.85), channel_id=1, source_target_pairs={{0,24},{8,16},{16,8},{24,0},{1,25},{9,17},{17,9},{25,1},{2,26},{10... | collective-permute-start | bytes 393224 | tf_op jit(solution)/shard_map/ppermute | solution.py:92
  139.8 17.7 %collective-permute-start.45 = (bf16[256,256]{1,0:T(8,128)(2,1)S(1)}, bf16[256,256]{1,0:T(8,128)(2,1)S(1)}, u32[]{:S(2)}, u32[]{:S(2)}) collective-permute-start(bf16[256,256]{1,0:T(8,128)(2,1)S(1)} %get-tuple-element.84), channel_id=1, source_target_pairs={{0,16},{8,24},{16,0},{24,8},{1,17},{9,25},{17,1},{25,9},{2,18},{10... | collective-permute-start | bytes 393224 | tf_op jit(solution)/shard_map/ppermute | solution.py:92
  141.2 16.3 %collective-permute-start.44 = (bf16[256,256]{1,0:T(8,128)(2,1)S(1)}, bf16[256,256]{1,0:T(8,128)(2,1)S(1)}, u32[]{:S(2)}, u32[]{:S(2)}) collective-permute-start(bf16[256,256]{1,0:T(8,128)(2,1)S(1)} %get-tuple-element.83), channel_id=1, source_target_pairs={{0,8},{8,0},{16,24},{24,16},{1,9},{9,1},{17,25},{25,17},{2,10},{10... | collective-permute-start | bytes 393224 | tf_op jit(solution)/shard_map/ppermute | solution.py:92
  (40 other events, 317.5 us)
